TPU v7x, 32 devices: a whole 2x2x4 slice. The times are simulated.
32 devices in a mesh: sp: 8 (over z, x), dp: 4 (over y, core).
Axes of the slice: x: 2, y: 2, z: 4, core: 2. Of those that a mesh axis runs over, the one named last changes fastest.
Arguments:
- queries: bfloat16 [4, 1024, 16, 128], P('dp', 'sp'), may hold values from -6 to 6
- key_rows: bfloat16 [4, 1024, 4, 128], P('dp', 'sp'), may hold values from -6 to 6
- values: bfloat16 [4, 1024, 4, 128], P('dp', 'sp'), may hold values from -6 to 6
- query_gain: float32 [128], replicated, may hold values from 0.4 to 5
- key_gain: float32 [128], replicated, may hold values from 0.4 to 5
- out_weight: bfloat16 [2048, 2048], P('sp', 'dp'), may hold values from -0.125 to 0.125
- residual: bfloat16 [4, 1024, 2048], P('dp', 'sp'), may hold values from -6 to 6
- norm_gain: float32 [2048], replicated, may hold values from 0.1 to 1.9
- expert_gate: bfloat16 [8, 2048, 1792], P('sp'), may hold values from -0.125 to 0.125
- expert_up: bfloat16 [8, 2048, 1792], P('sp'), may hold values from -0.125 to 0.125
- expert_down: bfloat16 [8, 1792, 2048], P('sp'), may hold values from -0.125 to 0.125
- routes: int32 [4, 1024, 2], P('dp', 'sp'), may hold values from 0 to 7, all different within a row; in each aligned block of 64 rows (0 to 63, 64 to 127, ..., all dimensions but the last counted through in order) at most 32 rows name the same one
- route_weight: float32 [4, 1024, 2], P('dp', 'sp'), may hold values from 0.25 to 1
Outputs:
- layer_out: bfloat16 [4, 1024, 2048], P('dp', 'sp')
Inputs may be any that keep to these rules, and one draw needn't show every extreme that they name: `routes`: in each aligned block of 64 rows of one device, no expert is named by more than 32 entries, a bound that some block reaches; the two experts of a row differ.
All inputs are finite; a program needn't handle non-finite values.
Results may differ from a plain program's by a relative error of at most 0.0095.
The roundings to bfloat16 on the way count: a program that leaves them out, or rounds other values in their place, can miss the bound.
Values may be sent and summed in bfloat16 or wider, within the bound.
A program may use at most 128 MiB of HBM per device.

v0:
```python
import functools

import jax
import jax.numpy as jnp
from jax import lax
from jax.experimental import pallas as pl
from jax.experimental.pallas import tpu as pltpu
from jax.sharding import PartitionSpec as P

GRID_W = 64
EPS = 1e-06
THETA = 10000.0
MESH = pl.DeviceIdType.MESH
VMEM = pl.BlockSpec(memory_space=pltpu.VMEM)
ANY = pl.BlockSpec(memory_space=pl.ANY)
F32 = jnp.float32
BF16 = jnp.bfloat16


def rotation_tables(positions, head_width):
    quarter = head_width // 4
    inverse = THETA ** (-jnp.arange(quarter, dtype=F32) / quarter)
    grid_row = (positions // GRID_W).astype(F32)[:, None] * inverse[None, :]
    column = (positions % GRID_W).astype(F32)[:, None] * inverse[None, :]
    angles = jnp.concatenate([grid_row, grid_row, column, column], axis=-1)
    lane = jnp.arange(head_width) % (2 * quarter)
    sign = jnp.where(lane < quarter, -1.0, 1.0).astype(F32)
    return jnp.cos(angles), jnp.sin(angles) * sign[None, :]


def turn(rows, gain, cosine, sine):
    width = rows.shape[-1]
    quarter = width // 4
    a = rows.astype(F32)
    a = a * lax.rsqrt(jnp.mean(a * a, axis=-1, keepdims=True) + EPS) * gain
    lane = lax.broadcasted_iota(jnp.int32, a.shape, 1) % (2 * quarter)
    partner = jnp.where(
        lane < quarter, pltpu.roll(a, width - quarter, 1), pltpu.roll(a, quarter, 1)
    )
    return (a * cosine + partner * sine).astype(BF16)


class Spread:
    def __init__(self, n, block, send, recv, z_first):
        self.width = max(x for x in range(1, n + 1) if n % x == 0 and x * x <= n)
        self.depth = n // self.width
        self.block, self.send, self.recv, self.z_first = block, send, recv, z_first
        me = lax.axis_index("sp")
        self.z, self.x = me // self.width, me % self.width
        self.ends = []

    def copy(self, source, way, target):
        return pltpu.make_async_remote_copy(
            src_ref=self.block(source),
            dst_ref=self.block(source),
            send_sem=self.send.at[source, way],
            recv_sem=self.recv.at[source],
            device_id={"sp": target},
            device_id_type=MESH,
        )

    def at(self, z, x):
        return z * self.width + x

    def start(self, condition, source, way, target):
        @pl.when(condition)
        def _():
            self.copy(source, way, target).start()

        self.ends.append((condition, source, way, target))

    def up(self, condition, source):
        ok = condition & (self.z < self.depth - 1)
        self.start(ok, source, 0, self.at(self.z + 1, self.x))

    def down(self, condition, source):
        ok = condition & (self.z > 0)
        self.start(ok, source, 1, self.at(self.z - 1, self.x))

    def across(self, condition, source):
        for k in range(1, self.width):
            self.start(condition, source, 1 + k, self.at(self.z, (self.x + k) % self.width))

    def arrive(self, condition, source):
        @pl.when(condition)
        def _():
            self.copy(source, 0, source).wait_recv()

    def columns(self):
        if self.z_first:
            return [self.x]
        return [(self.x + k) % self.width for k in range(self.width)]

    def begin(self):
        own = self.at(self.z, self.x)
        always = self.z >= 0
        if not self.z_first:
            self.across(always, own)
        self.up(always, own)
        self.down(always, own)
        if self.z_first:
            self.across(always, own)

    def second(self):
        always = self.z >= 0
        for x in self.columns()[1:]:
            source = self.at(self.z, x)
            self.arrive(always, source)
            self.up(always, source)
            self.down(always, source)

    def step(self, t):
        for x in self.columns():
            below, above = self.z - t >= 0, self.z + t < self.depth
            source = self.at(self.z - t, x)
            self.arrive(below, source)
            self.up(below, source)
            if self.z_first:
                self.across(below, source)
            source = self.at(self.z + t, x)
            self.arrive(above, source)
            self.down(above, source)
            if self.z_first:
                self.across(above, source)

    def finish(self):
        always = self.z >= 0
        for z in range(self.depth):
            for k in range(1, self.width):
                self.arrive(always, self.at(z, (self.x + k) % self.width))

    def drain(self):
        for condition, source, way, target in self.ends:

            @pl.when(condition)
            def _():
                self.copy(source, way, target).wait_send()


def slot_choice(table, base, slots, capacity):
    rows = table.shape[0]
    slot = lax.broadcasted_iota(jnp.int32, (rows, slots), 1)
    expert = (slot // capacity + base).astype(F32)
    first = table[:, 0:1] == expert
    second = table[:, 1:2] == expert
    named = jnp.where(first | second, 1.0, 0.0).astype(BF16)
    earlier = lax.broadcasted_iota(jnp.int32, (rows, rows), 1) < lax.broadcasted_iota(
        jnp.int32, (rows, rows), 0
    )
    rank = jnp.dot(
        jnp.where(earlier, 1.0, 0.0).astype(BF16), named, preferred_element_type=F32
    )
    here = rank == (slot % capacity).astype(F32)
    return (
        jnp.where(first & here, 1.0, 0.0).astype(BF16),
        jnp.where(second & here, 1.0, 0.0).astype(BF16),
    )


def attention_part(
    n,
    dp,
    start_loads,
    q_ref,
    k_ref,
    v_ref,
    qg_ref,
    kg_ref,
    cos_ref,
    sin_ref,
    w_ref,
    res_ref,
    ng_ref,
    table_ref,
    mixed_ref,
    normed_ref,
    table,
    q_rot,
    kv,
    w_full,
    att,
    proj,
    back,
    res_in,
    gains,
    norm_in,
    in_sem,
    x_send,
    x_recv,
    t_sem,
    y_send,
    y_recv,
    pair_send,
    pair_recv,
    fwd_send,
    fwd_recv,
    back_send,
    back_recv,
):
    me = lax.axis_index("sp")
    mine = lax.axis_index("dp")
    heads, rows, width = q_ref.shape
    kv_heads = k_ref.shape[0]
    group = heads // kv_heads
    model = heads * width
    ny = dp // 2
    core = mine % 2
    row_y = mine // 2
    partner = row_y * 2 + 1 - core

    w_rows = w_ref.shape[0]
    my_w = pl.ds(pl.multiple_of(me * w_rows, w_rows), w_rows)
    fetches = [
        pltpu.make_async_copy(src, dst, in_sem.at[i])
        for i, (src, dst) in enumerate(
            (
                (kg_ref, gains.at[0]),
                (qg_ref, gains.at[1]),
                (w_ref, w_full.at[my_w]),
                (res_ref, res_in),
                (ng_ref, norm_in),
            )
        )
    ]
    for fetch in fetches:
        fetch.start()
    barrier = pltpu.get_barrier_semaphore()
    for d in range(1, n):
        pl.semaphore_signal(
            barrier, inc=1, device_id={"sp": lax.rem(me + d, n)}, device_id_type=MESH
        )
    for d in range(1, dp):
        pl.semaphore_signal(
            barrier, inc=1, device_id={"dp": lax.rem(mine + d, dp)}, device_id_type=MESH
        )

    cosine = cos_ref[...]
    sine = sin_ref[...]
    my_rows = pl.ds(pl.multiple_of(me * rows, rows), rows)
    fetches[0].wait()
    for g in range(kv_heads):
        kv[g, my_rows, :] = turn(k_ref[g], gains[0], cosine, sine)
        kv[kv_heads + g, my_rows, :] = v_ref[g]
    pl.semaphore_wait(barrier, n - 1 + dp - 1)

    def key_block(s):
        return kv.at[pl.ds(0, kv_heads), pl.ds(pl.multiple_of(s * rows, rows), rows), :]

    def value_block(s):
        return kv.at[pl.ds(kv_heads, kv_heads), pl.ds(pl.multiple_of(s * rows, rows), rows), :]

    def weight_block(part):
        size = w_rows // 2
        return lambda s: w_full.at[
            pl.ds(pl.multiple_of(s * w_rows + part * size, size), size)
        ]

    attention_gather = (
        Spread(n, value_block, x_send.at[0], x_recv.at[0], False),
        Spread(n, key_block, x_send.at[1], x_recv.at[1], True),
    )
    weight_gather = (
        Spread(n, weight_block(1), x_send.at[2], x_recv.at[2], False),
        Spread(n, weight_block(0), x_send.at[3], x_recv.at[3], True),
    )
    table_copy = pltpu.make_async_remote_copy(
        src_ref=table_ref,
        dst_ref=table,
        send_sem=t_sem.at[0],
        recv_sem=t_sem.at[1],
        device_id={"sp": lax.rem(me + n // 2, n)},
        device_id_type=MESH,
    )
    table_copy.start()
    for spread in attention_gather:
        spread.begin()

    start_loads()
    fetches[1].wait()

    def turn_head(h, carry):
        q_rot[h] = turn(q_ref[h], gains[1], cosine, sine)
        return carry

    lax.fori_loop(0, heads, turn_head, 0)
    attention_gather[0].second()
    steps = attention_gather[0].depth
    for t in range(1, steps):
        for spread in attention_gather:
            spread.step(t)
        if t == 1:
            fetches[2].wait()
            for spread in weight_gather:
                spread.begin()
    attention_gather[1].finish()

    per_step = 2
    scale = width ** (-0.5)
    pair_copies = []
    y_copies = {}
    for g in range(kv_heads):

        def some_heads(i, carry):
            first = g * group + i * per_step
            query = q_rot[pl.ds(first, per_step)].reshape(per_step * rows, width)
            scores = (
                lax.dot_general(
                    query, kv[g], (((1,), (1,)), ((), ())), preferred_element_type=F32
                )
                * scale
            )
            exponent = jnp.exp(scores - jnp.max(scores, axis=-1, keepdims=True))
            weights = (exponent / jnp.sum(exponent, axis=-1, keepdims=True)).astype(BF16)
            out = jnp.dot(weights, kv[kv_heads + g], preferred_element_type=F32).astype(BF16)
            for j in range(per_step):
                cols = pl.ds(pl.multiple_of((first + j) * width, width), width)
                att[mine, :, cols] = out[j * rows : (j + 1) * rows]
            return carry

        lax.fori_loop(0, group // per_step, some_heads, 0)
        cols = slice(g * group * width, (g + 1) * group * width)
        for j in range(1, ny):
            copy = pltpu.make_async_remote_copy(
                src_ref=att.at[mine, :, cols],
                dst_ref=att.at[mine, :, cols],
                send_sem=y_send.at[j, g],
                recv_sem=y_recv.at[j, g],
                device_id={"dp": lax.rem(row_y + j, ny) * 2 + core},
                device_id_type=MESH,
            )
            copy.start()
            y_copies[j, g] = copy
        copy = pltpu.make_async_remote_copy(
            src_ref=att.at[mine, :, cols],
            dst_ref=att.at[mine, :, cols],
            send_sem=pair_send.at[g],
            recv_sem=pair_recv.at[g],
            device_id={"dp": partner},
            device_id_type=MESH,
        )
        copy.start()
        pair_copies.append(copy)
        if g == 0:
            weight_gather[0].second()

    for t in range(1, steps):
        for spread in weight_gather:
            spread.step(t)
    weight_gather[1].finish()
    fwd_copies = {}

    def forward(j):
        source = lax.rem(row_y + ny - j, ny) * 2 + core
        for g in range(kv_heads):
            cols = slice(g * group * width, (g + 1) * group * width)
            y_copies[j, g].wait_recv()
            copy = pltpu.make_async_remote_copy(
                src_ref=att.at[source, :, cols],
                dst_ref=att.at[source, :, cols],
                send_sem=fwd_send.at[j, g],
                recv_sem=fwd_recv.at[j, g],
                device_id={"dp": partner},
                device_id_type=MESH,
            )
            copy.start()
            fwd_copies[j, g] = copy
        return source

    def project(seq):
        return jnp.dot(att[seq], w_full[...], preferred_element_type=F32).astype(BF16)

    back_copies = []

    def send_back(seq, index):
        proj[index] = project(seq)
        copy = pltpu.make_async_remote_copy(
            src_ref=proj.at[index],
            dst_ref=back.at[mine],
            send_sem=back_send.at[index],
            recv_sem=back_recv.at[index],
            device_id={"dp": seq},
            device_id_type=MESH,
        )
        copy.start()
        back_copies.append(copy)

    index = 1
    back[mine] = project(mine)
    for copy in pair_copies:
        copy.wait_recv()
    send_back(partner, index)
    index += 1
    for j in range(1, ny):
        source = forward(j)
        send_back(source, index)
        index += 1
        for g in range(kv_heads):
            fwd_copies[j, g].wait_recv()
        send_back(lax.rem(row_y + ny - j, ny) * 2 + 1 - core, index)
        index += 1

    for spread in attention_gather + weight_gather:
        spread.drain()
    table_copy.wait()
    fetches[3].wait()
    fetches[4].wait()
    for copy in pair_copies:
        copy.wait_send()
    for j in range(1, ny):
        for g in range(kv_heads):
            y_copies[j, g].wait_send()
            fwd_copies[j, g].wait_send()
    for copy in back_copies:
        copy.wait()
    block = w_ref.shape[1]
    square = jnp.zeros((rows, 1), F32)
    for s in range(dp):
        cols = slice(s * block, (s + 1) * block)
        part = res_in[:, cols].astype(F32) + back[s].astype(F32)
        mixed_ref[:, cols] = part
        square = square + jnp.sum(part * part, axis=-1, keepdims=True)
    factor = lax.rsqrt(square / model + EPS)
    for s in range(dp):
        cols = slice(s * block, (s + 1) * block)
        normed_ref[:, cols] = (mixed_ref[:, cols] * factor * norm_in[:, cols]).astype(BF16)


def expert_part(
    n,
    capacity,
    normed_ref,
    mixed_ref,
    own_ref,
    other_ref,
    loads,
    out_ref,
    gate,
    up,
    down,
    relay,
    sent,
    recv,
    hidden,
    res,
    ret,
    part,
    home,
    hold,
    relay_sem,
    home_sem,
    go_send,
    go_recv,
    ret_send,
    ret_recv,
):
    me = lax.axis_index("sp")
    half = n // 2
    base = me // half * half
    mine = me % half
    partner = lax.rem(me + half, n)
    rows, model = normed_ref.shape
    few = rows // 2
    slots = half * capacity
    ff = gate.shape[1]

    def peer(k):
        return base + lax.rem(mine + k, half)

    relays = []
    for b in range(2):
        copy = pltpu.make_async_remote_copy(
            src_ref=normed_ref.at[pl.ds(b * few, few)],
            dst_ref=relay.at[b],
            send_sem=relay_sem.at[0, b],
            recv_sem=relay_sem.at[1, b],
            device_id={"sp": partner},
            device_id_type=MESH,
        )
        copy.start()
        relays.append(copy)

    def block(index):
        return pl.ds(pl.multiple_of(index * capacity, capacity), capacity)

    go, back, homes = {}, {}, []

    def choices(r):
        table = own_ref if r < 2 else other_ref
        return slot_choice(table[(r % 2) * few : (r % 2 + 1) * few], base, slots, capacity)

    def dispatch(r):
        first, second = choices(r)
        choice = first + second
        lines = normed_ref[(r % 2) * few : (r % 2 + 1) * few] if r < 2 else relay[r % 2]
        for t in range(model // 512):
            cols = slice(t * 512, (t + 1) * 512)
            sent[r, :, cols] = lax.dot_general(
                choice, lines[:, cols], (((0,), (0,)), ((), ())), preferred_element_type=F32
            ).astype(BF16)
        recv[r, block(mine)] = sent[r, block(mine)]
        for k in range(1, half):
            copy = pltpu.make_async_remote_copy(
                src_ref=sent.at[r, block(lax.rem(mine + k, half))],
                dst_ref=recv.at[r, block(mine)],
                send_sem=go_send.at[r, k],
                recv_sem=go_recv.at[r, k],
                device_id={"sp": peer(k)},
                device_id_type=MESH,
            )
            copy.start()
            go[r, k] = copy

    tile = 256

    def serve(r):
        for k in range(1, half):
            go[r, k].wait_recv()

        def up_tile(t, carry):
            cols = pl.ds(pl.multiple_of(t * tile, tile), tile)
            gate_part = jnp.dot(recv[r], gate[:, cols], preferred_element_type=F32)
            up_part = jnp.dot(recv[r], up[:, cols], preferred_element_type=F32)
            hidden[:, cols] = (gate_part / (1.0 + jnp.exp(-gate_part)) * up_part).astype(BF16)
            return carry

        lax.fori_loop(0, ff // tile, up_tile, 0)
        if r == 0:
            loads[2].wait()

        def down_tile(t, carry):
            cols = pl.ds(pl.multiple_of(t * tile, tile), tile)
            res[r, :, cols] = jnp.dot(
                hidden[...], down[:, cols], preferred_element_type=F32
            ).astype(BF16)
            return carry

        lax.fori_loop(0, model // tile, down_tile, 0)
        ret[r, block(mine)] = res[r, block(mine)]
        for k in range(1, half):
            copy = pltpu.make_async_remote_copy(
                src_ref=res.at[r, block(lax.rem(mine + k, half))],
                dst_ref=ret.at[r, block(mine)],
                send_sem=ret_send.at[r, k],
                recv_sem=ret_recv.at[r, k],
                device_id={"sp": peer(k)},
                device_id_type=MESH,
            )
            copy.start()
            back[r, k] = copy

    def combine(r, store):
        first, second = choices(r)
        table = own_ref if r < 2 else other_ref
        lines = slice((r % 2) * few, (r % 2 + 1) * few)
        for k in range(1, half):
            back[r, k].wait_recv()
        for t in range(model // 512):
            cols = slice(t * 512, (t + 1) * 512)
            served = ret[r, :, cols]
            store(
                lines,
                cols,
                jnp.dot(first, served, preferred_element_type=F32) * table[lines, 2:3]
                + jnp.dot(second, served, preferred_element_type=F32) * table[lines, 3:4],
            )

    def store_part(lines, cols, value):
        part[lines, cols] = value.astype(BF16)

    def send_home(b):
        combine(2 + b, store_part)
        copy = pltpu.make_async_remote_copy(
            src_ref=part.at[pl.ds(b * few, few)],
            dst_ref=home.at[b],
            send_sem=home_sem.at[0, b],
            recv_sem=home_sem.at[1, b],
            device_id={"sp": partner},
            device_id_type=MESH,
        )
        copy.start()
        homes.append(copy)

    def store_own(lines, cols, value):
        hold[lines, cols] = mixed_ref[lines, cols] + value

    dispatch(0)
    dispatch(1)
    loads[0].wait()
    loads[1].wait()
    serve(0)
    relays[0].wait_recv()
    dispatch(2)
    serve(1)
    relays[1].wait_recv()
    dispatch(3)
    serve(2)
    serve(3)
    send_home(0)
    send_home(1)
    combine(0, store_own)
    combine(1, store_own)
    for b in range(2):
        homes[b].wait_recv()
        lines = slice(b * few, (b + 1) * few)
        out_ref[lines] = (hold[lines] + home[b].astype(F32)).astype(BF16)
    for b in range(2):
        relays[b].wait_send()
        homes[b].wait_send()
    for r in range(4):
        for k in range(1, half):
            go[r, k].wait_send()
            back[r, k].wait_send()


def layer_kernel(n, dp, capacity, *refs):
    inputs, refs = refs[:11], refs[11:]
    weights, out_ref, refs = refs[:3], refs[3], refs[4:]
    middle, refs = refs[:3], refs[3:]
    attention, refs = refs[:21], refs[21:]
    load_sem, stores, experts = refs[0], refs[1:4], refs[4:]
    loads = [
        pltpu.make_async_copy(src.at[0], dst, load_sem.at[i])
        for i, (src, dst) in enumerate(zip(weights, stores))
    ]

    def start_loads():
        for load in loads:
            load.start()

    attention_part(n, dp, start_loads, *inputs, *middle, *attention)
    mixed, normed, other = middle
    expert_part(n, capacity, normed, mixed, inputs[10], other, loads, out_ref, *stores, *experts)


def on_device(
    n,
    dp,
    queries,
    key_rows,
    values,
    query_gain,
    key_gain,
    out_weight,
    residual,
    norm_gain,
    expert_gate,
    expert_up,
    expert_down,
    routes,
    route_weight,
):
    _, rows, heads, width = queries.shape
    kv_heads = key_rows.shape[2]
    model = heads * width
    length = rows * n
    experts = expert_gate.shape[0] * n
    capacity = max(2, 4 * (rows // 2) // experts)
    slots = n // 2 * capacity
    table = jnp.concatenate([routes[0].astype(F32), route_weight[0]], axis=-1)
    table = jnp.pad(table, ((0, 0), (0, width - table.shape[1])))
    x_width = max(x for x in range(1, n + 1) if n % x == 0 and x * x <= n)
    positions = lax.axis_index("sp") * rows + jnp.arange(rows, dtype=jnp.int32)
    cosine, sine = rotation_tables(positions, width)
    w_rows, w_cols = out_weight.shape
    dma = pltpu.SemaphoreType.DMA
    ny = dp // 2
    ff = expert_gate.shape[2]
    few = rows // 2
    attention_scratch = [
        pltpu.VMEM((heads, rows, width), BF16),
        pltpu.VMEM((2 * kv_heads, length, width), BF16),
        pltpu.VMEM((w_rows * n, w_cols), BF16),
        pltpu.VMEM((dp, rows, model), BF16),
        pltpu.VMEM((dp, rows, w_cols), BF16),
        pltpu.VMEM((dp, rows, w_cols), BF16),
        pltpu.VMEM((rows, model), BF16),
        pltpu.VMEM((2, 1, width), F32),
        pltpu.VMEM((1, model), F32),
        dma((5,)),
        dma((4, n, 1 + x_width)),
        dma((4, n)),
        dma((2,)),
        dma((ny, kv_heads)),
        dma((ny, kv_heads)),
        dma((kv_heads,)),
        dma((kv_heads,)),
        dma((ny, kv_heads)),
        dma((ny, kv_heads)),
        dma((dp,)),
        dma((dp,)),
    ]
    result = pl.pallas_call(
        functools.partial(layer_kernel, n, dp, capacity),
        out_shape=jax.ShapeDtypeStruct((rows, model), BF16),
        in_specs=[VMEM, VMEM, VMEM, ANY, ANY, VMEM, VMEM, ANY, ANY, ANY, VMEM] + [ANY] * 3,
        out_specs=VMEM,
        scratch_shapes=[
            pltpu.VMEM((rows, model), F32),
            pltpu.VMEM((rows, model), BF16),
            pltpu.VMEM(table.shape, F32),
            *attention_scratch,
            dma((3,)),
            pltpu.VMEM((model, ff), BF16),
            pltpu.VMEM((model, ff), BF16),
            pltpu.VMEM((ff, model), BF16),
            pltpu.VMEM((2, few, model), BF16),
            pltpu.VMEM((4, slots, model), BF16),
            pltpu.VMEM((4, slots, model), BF16),
            pltpu.VMEM((slots, ff), BF16),
            pltpu.VMEM((4, slots, model), BF16),
            pltpu.VMEM((4, slots, model), BF16),
            pltpu.VMEM((rows, model), BF16),
            pltpu.VMEM((2, few, model), BF16),
            pltpu.VMEM((rows, model), F32),
            dma((2, 2)),
            dma((2, 2)),
            dma((4, n)),
            dma((4, n)),
            dma((4, n)),
            dma((4, n)),
        ],
        compiler_params=pltpu.CompilerParams(
            collective_id=0, has_side_effects=True, vmem_limit_bytes=56 * 1024 * 1024
        ),
        name="layer",
    )(
        queries[0].transpose(1, 0, 2),
        key_rows[0].transpose(1, 0, 2),
        values[0].transpose(1, 0, 2),
        query_gain[None],
        key_gain[None],
        cosine,
        sine,
        out_weight,
        residual[0],
        norm_gain[None],
        table,
        expert_gate,
        expert_up,
        expert_down,
    )
    return result[None]


def solution(mesh):
    in_specs = (
        P("dp", "sp", None, None),
        P("dp", "sp", None, None),
        P("dp", "sp", None, None),
        P(),
        P(),
        P("sp", "dp"),
        P("dp", "sp", None),
        P(),
        P("sp", None, None),
        P("sp", None, None),
        P("sp", None, None),
        P("dp", "sp", None),
        P("dp", "sp", None),
    )
    out_specs = P("dp", "sp", None)
    return jax.shard_map(
        functools.partial(on_device, mesh.shape["sp"], mesh.shape["dp"]),
        mesh=mesh,
        in_specs=in_specs,
        out_specs=out_specs,
        check_vma=False,
    )
```

profile of v0, /device:TPU:8, one launch (start us, length us, event | category | flops | bytes accessed | tf_op | source)
XLA Modules:
  0.0 162.1 jit_solution(4983028714243170640)
XLA Ops:
  0.0 0.7 convert_bitcast_fusion
  0.7 0.7 pad_maximum_fusion.1
  1.4 0.1 copy.22
  1.5 0.6 pad.4.refs_10_
  2.2 0.1 broadcast_multiply_fusion.1
  2.3 1.0 sine_multiply_fusion
  3.3 1.7 %copy_bitcast_fusion.1 = (bf16[4,128,128]{2,1,0:T(8,128)(2,1)}, bf16[4,128,128]{2,1,0:T(8,128)(2,1)}) fusion(bf16[1,128,4,128]{3,2,1,0:T(4,128)(2,1)} %param.15, bf16[1,128,4,128]{3,2,1,0:T(4,128)(2,1)} %param.14), kind=kLoop, calls=%fused_computation.1 | loop fusion | bytes 524288 | tf_op jit(solution)/shard_map/transpose | solution.py:729
  5.0 2.0 %copy.26 = bf16[1,128,16,128]{3,1,2,0:T(8,128)(2,1)} copy(bf16[1,128,16,128]{3,2,1,0:T(8,128)(2,1)} %param.13) | data formatting | bytes 1048576 | tf_op args[0]
  6.9 153.3 %layer.1 = bf16[128,2048]{1,0:T(8,128)(2,1)} custom-call(bf16[16,128,128]{2,1,0:T(8,128)(2,1)} %bitcast.22, bf16[4,128,128]{2,1,0:T(8,128)(2,1)} %get-tuple-element.12.refs_1_, bf16[4,128,128]{2,1,0:T(8,128)(2,1)} %get-tuple-element.11.refs_2_, f32[1,128]{1,0:T(1,128)} %bitcast.26, f32[1,128]{1,0:T(1,128)} %bitcast.27, f32[128,128]{1,0:T(8,128)} %get-tuple-element.6.refs_5_, ...), custom_call_target="tpu_custom_call" | custom-call | tf_op jit(solution)/shard_map/layer/pallas_call | solution.py:692
  160.2 1.9 %copy.28 = bf16[1,128,2048]{2,1,0:T(8,128)(2,1)} copy(bf16[1,128,2048]{2,1,0:T(8,128)(2,1)} %bitcast.21) | data formatting | bytes 1048576
  (3 shorter events, 0.0 us)
where the time goes:
time: 164 us; the launch traced here: 162 us
  Pallas kernels  153 us (93%)
  local copies, waits for them, and re-layouts  6.3 us (4%)
  other arithmetic  2.49 us (2%)
    pallas_call x1, Pallas kernels, on_device(): pl.pallas_call(functools.partial(layer_kernel, n, dp, capacity), out_shap...  153 us
    unnamed x2, local copies, waits for them, and re-layouts  3.85 us

commit v1 on v0

v1 whole, which is shorter than its diff:
```python
import functools
import math

import jax
import jax.numpy as jnp
from jax import lax
from jax.experimental import pallas as pl
from jax.experimental.pallas import tpu as pltpu
from jax.sharding import PartitionSpec as P

GRID_W = 64
EPS = 1e-06
THETA = 10000.0
MESH = pl.DeviceIdType.MESH
VMEM = pl.BlockSpec(memory_space=pltpu.VMEM)
ANY = pl.BlockSpec(memory_space=pl.ANY)
F32 = jnp.float32
BF16 = jnp.bfloat16


def rotation_tables(start, rows, width):
    quarter = width // 4
    lane = lax.broadcasted_iota(jnp.int32, (rows, width), 1)
    position = start + lax.broadcasted_iota(jnp.int32, (rows, width), 0)
    place = jnp.where(lane < 2 * quarter, position // GRID_W, position % GRID_W)
    part = lane % (2 * quarter)
    power = (part % quarter).astype(F32) * (-math.log(THETA) / quarter)
    angles = place.astype(F32) * jnp.exp(power)
    sign = jnp.where(part < quarter, -1.0, 1.0).astype(F32)
    return jnp.cos(angles), jnp.sin(angles) * sign


def turn(rows, gain, cosine, sine):
    width = rows.shape[-1]
    quarter = width // 4
    a = rows.astype(F32)
    a = a * lax.rsqrt(jnp.mean(a * a, axis=-1, keepdims=True) + EPS) * gain
    lane = lax.broadcasted_iota(jnp.int32, a.shape, 1) % (2 * quarter)
    partner = jnp.where(
        lane < quarter, pltpu.roll(a, width - quarter, 1), pltpu.roll(a, quarter, 1)
    )
    return (a * cosine + partner * sine).astype(BF16)


class Line:
    def __init__(self, depth, width, block, send, recv):
        self.depth, self.width, self.block = depth, width, block
        self.send, self.recv = send, recv
        me = lax.axis_index("sp")
        self.z, self.x = me // width, me % width
        self.ends = []

    def copy(self, unit, plane, way, target):
        return pltpu.make_async_remote_copy(
            src_ref=self.block(unit, plane * self.width + self.x),
            dst_ref=self.block(unit, plane * self.width + self.x),
            send_sem=self.send.at[unit, plane, way],
            recv_sem=self.recv.at[unit, plane],
            device_id={"sp": target * self.width + self.x},
            device_id_type=MESH,
        )

    def start(self, condition, unit, plane, way, target):
        @pl.when(condition)
        def _():
            self.copy(unit, plane, way, target).start()

        self.ends.append((condition, unit, plane, way, target))

    def up(self, condition, unit, plane):
        self.start(condition & (self.z < self.depth - 1), unit, plane, 0, self.z + 1)

    def down(self, condition, unit, plane):
        self.start(condition & (self.z > 0), unit, plane, 1, self.z - 1)

    def arrive(self, condition, unit, plane):
        @pl.when(condition)
        def _():
            self.copy(unit, plane, 0, plane).wait_recv()

    def step(self, t, unit, condition=True, then=None):
        below = (self.z - t >= 0) & condition
        above = (self.z + t < self.depth) & condition
        self.arrive(below, unit, self.z - t)
        self.up(below, unit, self.z - t)
        if then is not None:
            then(below, unit, self.z - t)
        self.arrive(above, unit, self.z + t)
        self.down(above, unit, self.z + t)
        if then is not None:
            then(above, unit, self.z + t)

    def drain(self):
        for condition, unit, plane, way, target in self.ends:

            @pl.when(condition)
            def _():
                self.copy(unit, plane, way, target).wait_send()


def slot_choice(table, base, slots, capacity):
    rows = table.shape[0]
    slot = lax.broadcasted_iota(jnp.int32, (rows, slots), 1)
    expert = (slot // capacity + base).astype(F32)
    first = table[:, 0:1] == expert
    second = table[:, 1:2] == expert
    named = jnp.where(first | second, 1.0, 0.0).astype(BF16)
    earlier = lax.broadcasted_iota(jnp.int32, (rows, rows), 1) < lax.broadcasted_iota(
        jnp.int32, (rows, rows), 0
    )
    rank = jnp.dot(
        jnp.where(earlier, 1.0, 0.0).astype(BF16), named, preferred_element_type=F32
    )
    here = rank == (slot % capacity).astype(F32)
    return (
        jnp.where(first & here, 1.0, 0.0).astype(BF16),
        jnp.where(second & here, 1.0, 0.0).astype(BF16),
    )


def attention_part(
    n,
    dp,
    start_loads,
    q_ref,
    k_ref,
    v_ref,
    qg_ref,
    kg_ref,
    w_ref,
    res_ref,
    ng_ref,
    routes_ref,
    gates_ref,
    mixed_ref,
    normed_ref,
    own_table,
    table,
    q_in,
    k_in,
    v_in,
    wide,
    stage,
    q_stage,
    q_all,
    kv,
    w_full,
    swap,
    att,
    proj,
    back,
    res_in,
    gains,
    norm_in,
    in_sem,
    kvx_send,
    kvx_recv,
    kvz_send,
    kvz_recv,
    qx_send,
    qx_recv,
    wx_send,
    wx_recv,
    wz_send,
    wz_recv,
    ax_send,
    ax_recv,
    t_sem,
    y_send,
    y_recv,
    pair_send,
    pair_recv,
    fwd_send,
    fwd_recv,
    back_send,
    back_recv,
):
    me = lax.axis_index("sp")
    mine = lax.axis_index("dp")
    rows, heads, width = q_ref.shape
    kv_heads = k_ref.shape[1]
    group = heads // kv_heads
    model = heads * width
    across = stage.shape[0]
    depth = n // across
    local_kv = kv_heads // across
    local = heads // across
    z, x = me // across, me % across
    always = me >= 0
    ny = dp // 2
    core = mine % 2
    row_y = mine // 2
    partner = row_y * 2 + 1 - core
    w_rows, w_cols = w_ref.shape

    def span(start, size):
        return pl.ds(pl.multiple_of(start * size, size), size)

    fetches = [
        pltpu.make_async_copy(src, dst, in_sem.at[i])
        for i, (src, dst) in enumerate(
            (
                (k_ref, k_in),
                (v_ref, v_in),
                (kg_ref, gains.at[0]),
                (q_ref, q_in),
                (qg_ref, gains.at[1]),
                (w_ref, w_full.at[span(me, w_rows)]),
                (res_ref, res_in),
                (ng_ref, norm_in),
            )
        )
    ]
    for fetch in fetches:
        fetch.start()
    barrier = pltpu.get_barrier_semaphore()
    for d in range(1, n):
        pl.semaphore_signal(
            barrier, inc=1, device_id={"sp": lax.rem(me + d, n)}, device_id_type=MESH
        )
    for d in range(1, dp):
        pl.semaphore_signal(
            barrier, inc=1, device_id={"dp": lax.rem(mine + d, dp)}, device_id_type=MESH
        )

    cosine, sine = rotation_tables(me * rows, rows, width)
    my_rows = span(me, rows)
    for fetch in fetches[:3]:
        fetch.wait()
    for part, source in ((0, k_in), (1, v_in)):
        wide[:, 0:kv_heads, :] = source[...].astype(F32)
        for g in range(kv_heads):
            lines = wide[:, g, :]
            slot = 2 * (g % local_kv) + part
            if part == 0:
                lines = turn(lines, gains[0], cosine, sine)
            stage[g // local_kv, slot] = lines.astype(BF16)
    for c in range(2 * local_kv):
        kv[c, my_rows, :] = stage[x, c]
    pl.semaphore_wait(barrier, n - 1 + dp - 1)

    def remote(src, dst, send, recv, **device):
        return pltpu.make_async_remote_copy(
            src_ref=src,
            dst_ref=dst,
            send_sem=send,
            recv_sem=recv,
            device_id=device,
            device_id_type=MESH,
        )

    def beside(k):
        return z * across + lax.rem(x + k, across)

    def kv_block(g, sp):
        return kv.at[pl.ds(2 * g, 2), span(sp, rows), :]

    kv_units = [(k, g) for k in range(across) for g in range(local_kv)]

    def kv_unit(u, sp):
        k, g = kv_units[u]
        return kv_block(g, sp - sp % across + lax.rem(sp % across + k, across))

    halves = 2
    w_units = [(j, k) for j in range(halves) for k in range(2)]
    part_rows, part_cols = w_rows // 2, w_cols // halves

    def w_unit(u, sp):
        j, k = w_units[u]
        start = pl.multiple_of(sp * w_rows + k * part_rows, part_rows)
        return w_full.at[pl.ds(start, part_rows), pl.ds(j * part_cols, part_cols)]

    kv_line = Line(depth, across, kv_unit, kvz_send, kvz_recv)
    w_line = Line(depth, across, w_unit, wz_send, wz_recv)
    kvx, qx, ax, wx = {}, {}, {}, []
    for g in range(local_kv):
        for k in range(1, across):
            kvx[k, g] = remote(
                stage.at[lax.rem(x + k, across), pl.ds(2 * g, 2)],
                kv_block(g, me),
                kvx_send.at[k, g],
                kvx_recv.at[across - k, g],
                sp=beside(k),
            )
            kvx[k, g].start()
        kv_line.up(always, g, z)
        kv_line.down(always, g, z)

    start_loads()
    fetches[3].wait()
    fetches[4].wait()
    for h in range(0, heads, 8):
        wide[:, h : h + 8, :] = q_in[:, h : h + 8, :].astype(F32)
    for k in list(range(1, across)) + [0]:
        first = lax.rem(x + k, across) * local

        def turn_head(i, carry):
            lines = turn(wide[:, pl.ds(first + i, 1), :].reshape(rows, width), gains[1], cosine, sine)
            if k == 0:
                q_all[i, 0:rows] = lines
            else:
                q_stage[k - 1, i] = lines
            return carry

        lax.fori_loop(0, local, turn_head, 0)
        if k > 0:
            qx[k] = remote(
                q_stage.at[k - 1],
                q_all.at[:, pl.ds((across - k) * rows, rows), :],
                qx_send.at[k],
                qx_recv.at[across - k],
                sp=beside(k),
            )
            qx[k].start()
        if k == across - 1:
            for u in range(local_kv, len(kv_units)):
                kk, g = kv_units[u]
                remote(
                    stage.at[0, pl.ds(2 * g, 2)],
                    kv_block(g, beside(kk)),
                    kvx_send.at[kk, g],
                    kvx_recv.at[kk, g],
                    sp=me,
                ).wait_recv()
                kv_line.up(always, u, z)
                kv_line.down(always, u, z)
    fetches[5].wait()

    def w_across(condition, u, plane):
        for k in range(1, across):

            def copy():
                return remote(
                    w_unit(u, plane * across + x),
                    w_unit(u, plane * across + x),
                    wx_send.at[u, plane, k],
                    wx_recv.at[u, plane, across - k],
                    sp=beside(k),
                )

            @pl.when(condition)
            def _():
                copy().start()

            wx.append((condition, copy))

    def w_begin(t):
        for u in range(len(w_units)):
            w_line.up(z == t, u, z)
            w_line.down(depth - 1 - z == t, u, z)

    w_begin(0)
    lanes = jnp.concatenate(
        [
            routes_ref[...].astype(F32),
            gates_ref[...],
            jnp.zeros((width - 4, rows), F32),
        ],
        axis=0,
    )
    own_table[...] = lanes.T
    table_copy = remote(
        own_table, table, t_sem.at[0], t_sem.at[1], sp=lax.rem(me + n // 2, n)
    )
    table_copy.start()
    for u in range(len(w_units)):
        w_across(always, u, z)
    for t in range(1, depth):
        for u in range(len(kv_units)):
            kv_line.step(t, u)
        w_begin(t)
    middle = (z > 0) & (z < depth - 1)
    for u in range(len(w_units)):
        w_line.step(1, u, middle, w_across)
    for k in range(1, across):
        remote(
            q_stage.at[0],
            q_all.at[:, pl.ds(k * rows, rows), :],
            qx_send.at[k],
            qx_recv.at[k],
            sp=me,
        ).wait_recv()

    scale = width ** (-0.5)
    wide_group = group * width

    def att_cols(k, g):
        side = lax.rem(x + k, across)
        start = (side * local_kv + g) * wide_group
        return pl.ds(pl.multiple_of(start, wide_group), wide_group)

    y_copies, pair_copies, fwd_copies = {}, {}, {}

    def spread_att(u):
        k, g = kv_units[u]
        block = att.at[mine, :, att_cols(k, g)]
        for j in range(1, ny):
            target = lax.rem(row_y + j, ny) * 2 + core
            copy = remote(block, block, y_send.at[j, u], y_recv.at[j, u], dp=target)
            copy.start()
            y_copies[j, u] = copy
        copy = remote(block, block, pair_send.at[u], pair_recv.at[u], dp=partner)
        copy.start()
        pair_copies[u] = copy

    def forward(u):
        for j in range(1, ny):
            source = lax.rem(row_y + ny - j, ny) * 2 + core
            y_copies[j, u].wait_recv()
            block = att.at[source, :, att_cols(*kv_units[u])]
            copy = remote(block, block, fwd_send.at[j, u], fwd_recv.at[j, u], dp=partner)
            copy.start()
            fwd_copies[j, u] = copy

    for g in range(local_kv):

        def one_head(i, carry):
            h = g * group + i
            scores = (
                lax.dot_general(
                    q_all[h], kv[2 * g], (((1,), (1,)), ((), ())), preferred_element_type=F32
                )
                * scale
            )
            exponent = jnp.exp(scores - jnp.max(scores, axis=-1, keepdims=True))
            weights = (exponent / jnp.sum(exponent, axis=-1, keepdims=True)).astype(BF16)
            out = jnp.dot(weights, kv[2 * g + 1], preferred_element_type=F32).astype(BF16)
            cols = pl.ds(pl.multiple_of((x * local + h) * width, width), width)
            att[mine, :, cols] = out[0:rows]
            cols = pl.ds(pl.multiple_of(h * width, width), width)
            for k in range(1, across):
                swap[k - 1, :, cols] = out[k * rows : (k + 1) * rows]
            return carry

        lax.fori_loop(0, group, one_head, 0)
        for k in range(1, across):
            ax[k, g] = remote(
                swap.at[k - 1, :, pl.ds(g * wide_group, wide_group)],
                att.at[mine, :, att_cols(0, g)],
                ax_send.at[k, g],
                ax_recv.at[across - k, g],
                sp=beside(k),
            )
            ax[k, g].start()
        spread_att(g)
        if g == 0:
            for u in range(len(w_units)):
                w_line.step(1, u, jnp.logical_not(middle), w_across)
    for t in range(2, depth - 1):
        for u in range(len(w_units)):
            w_line.step(t, u, True, w_across)
    for u in range(local_kv, len(kv_units)):
        k, g = kv_units[u]
        remote(
            swap.at[0, :, pl.ds(g * wide_group, wide_group)],
            att.at[mine, :, att_cols(k, g)],
            ax_send.at[k, g],
            ax_recv.at[k, g],
            sp=me,
        ).wait_recv()
        spread_att(u)
    for u in range(len(kv_units)):
        forward(u)
    for u in range(len(w_units)):
        w_line.step(depth - 1, u, True, w_across)
    for u in range(len(kv_units)):
        pair_copies[u].wait_recv()
        for j in range(1, ny):
            fwd_copies[j, u].wait_recv()

    back_copies = {}
    for j in range(halves):
        for u, (jj, _) in enumerate(w_units):
            if jj != j:
                continue
            for plane in range(depth):
                for k in range(1, across):
                    remote(
                        w_unit(u, plane * across + x),
                        w_unit(u, plane * across + lax.rem(x + k, across)),
                        wx_send.at[u, plane, k],
                        wx_recv.at[u, plane, k],
                        sp=me,
                    ).wait_recv()
        cols = slice(j * part_cols, (j + 1) * part_cols)
        result = jnp.dot(
            att[...].reshape(dp * rows, model), w_full[:, cols], preferred_element_type=F32
        ).astype(BF16)
        for s in range(dp):
            proj[s, :, cols] = result[s * rows : (s + 1) * rows]
        back[mine, :, cols] = proj[mine, :, cols]
        order = sorted(range(1, dp), key=lambda d: d % 2)
        for d in order:
            target = lax.rem(mine + d, dp)
            copy = remote(
                proj.at[target, :, cols],
                back.at[mine, :, cols],
                back_send.at[d, j],
                back_recv.at[d, j],
                dp=target,
            )
            copy.start()
            back_copies[d, j] = copy

    kv_line.drain()
    w_line.drain()
    for condition, copy in wx:

        @pl.when(condition)
        def _():
            copy().wait_send()

    for copies in (kvx, qx, ax):
        for copy in copies.values():
            copy.wait_send()
    table_copy.wait()
    fetches[6].wait()
    fetches[7].wait()
    for copies in (y_copies, pair_copies, fwd_copies):
        for copy in copies.values():
            copy.wait_send()
    for copy in back_copies.values():
        copy.wait()
    square = jnp.zeros((rows, 1), F32)
    for s in range(dp):
        cols = slice(s * w_cols, (s + 1) * w_cols)
        part = res_in[:, cols].astype(F32) + back[s].astype(F32)
        mixed_ref[:, cols] = part
        square = square + jnp.sum(part * part, axis=-1, keepdims=True)
    factor = lax.rsqrt(square / model + EPS)
    for s in range(dp):
        cols = slice(s * w_cols, (s + 1) * w_cols)
        normed_ref[:, cols] = (mixed_ref[:, cols] * factor * norm_in[:, cols]).astype(BF16)


def expert_part(
    n,
    capacity,
    normed_ref,
    mixed_ref,
    own_ref,
    other_ref,
    loads,
    out_ref,
    gate,
    up,
    down,
    relay,
    sent,
    recv,
    hidden,
    res,
    ret,
    part,
    home,
    hold,
    relay_sem,
    home_sem,
    go_send,
    go_recv,
    ret_send,
    ret_recv,
):
    me = lax.axis_index("sp")
    half = n // 2
    base = me // half * half
    mine = me % half
    partner = lax.rem(me + half, n)
    rows, model = normed_ref.shape
    few = rows // 2
    slots = half * capacity
    ff = gate.shape[1]

    def peer(k):
        return base + lax.rem(mine + k, half)

    relays = []
    for b in range(2):
        copy = pltpu.make_async_remote_copy(
            src_ref=normed_ref.at[pl.ds(b * few, few)],
            dst_ref=relay.at[b],
            send_sem=relay_sem.at[0, b],
            recv_sem=relay_sem.at[1, b],
            device_id={"sp": partner},
            device_id_type=MESH,
        )
        copy.start()
        relays.append(copy)

    def block(index):
        return pl.ds(pl.multiple_of(index * capacity, capacity), capacity)

    go, back, homes = {}, {}, []

    def choices(r):
        table = own_ref if r < 2 else other_ref
        return slot_choice(table[(r % 2) * few : (r % 2 + 1) * few], base, slots, capacity)

    def dispatch(r):
        first, second = choices(r)
        choice = first + second
        lines = normed_ref[(r % 2) * few : (r % 2 + 1) * few] if r < 2 else relay[r % 2]
        for t in range(model // 512):
            cols = slice(t * 512, (t + 1) * 512)
            sent[r, :, cols] = lax.dot_general(
                choice, lines[:, cols], (((0,), (0,)), ((), ())), preferred_element_type=F32
            ).astype(BF16)
        recv[r, block(mine)] = sent[r, block(mine)]
        for k in range(1, half):
            copy = pltpu.make_async_remote_copy(
                src_ref=sent.at[r, block(lax.rem(mine + k, half))],
                dst_ref=recv.at[r, block(mine)],
                send_sem=go_send.at[r, k],
                recv_sem=go_recv.at[r, k],
                device_id={"sp": peer(k)},
                device_id_type=MESH,
            )
            copy.start()
            go[r, k] = copy

    tile = 256

    def serve(r):
        for k in range(1, half):
            go[r, k].wait_recv()

        def up_tile(t, carry):
            cols = pl.ds(pl.multiple_of(t * tile, tile), tile)
            gate_part = jnp.dot(recv[r], gate[:, cols], preferred_element_type=F32)
            up_part = jnp.dot(recv[r], up[:, cols], preferred_element_type=F32)
            hidden[:, cols] = (gate_part / (1.0 + jnp.exp(-gate_part)) * up_part).astype(BF16)
            return carry

        lax.fori_loop(0, ff // tile, up_tile, 0)
        if r == 0:
            loads[2].wait()

        def down_tile(t, carry):
            cols = pl.ds(pl.multiple_of(t * tile, tile), tile)
            res[r, :, cols] = jnp.dot(
                hidden[...], down[:, cols], preferred_element_type=F32
            ).astype(BF16)
            return carry

        lax.fori_loop(0, model // tile, down_tile, 0)
        ret[r, block(mine)] = res[r, block(mine)]
        for k in range(1, half):
            copy = pltpu.make_async_remote_copy(
                src_ref=res.at[r, block(lax.rem(mine + k, half))],
                dst_ref=ret.at[r, block(mine)],
                send_sem=ret_send.at[r, k],
                recv_sem=ret_recv.at[r, k],
                device_id={"sp": peer(k)},
                device_id_type=MESH,
            )
            copy.start()
            back[r, k] = copy

    def combine(r, store):
        first, second = choices(r)
        table = own_ref if r < 2 else other_ref
        lines = slice((r % 2) * few, (r % 2 + 1) * few)
        for k in range(1, half):
            back[r, k].wait_recv()
        for t in range(model // 512):
            cols = slice(t * 512, (t + 1) * 512)
            served = ret[r, :, cols]
            store(
                lines,
                cols,
                jnp.dot(first, served, preferred_element_type=F32) * table[lines, 2:3]
                + jnp.dot(second, served, preferred_element_type=F32) * table[lines, 3:4],
            )

    def store_part(lines, cols, value):
        part[lines, cols] = value.astype(BF16)

    def send_home(b):
        combine(2 + b, store_part)
        copy = pltpu.make_async_remote_copy(
            src_ref=part.at[pl.ds(b * few, few)],
            dst_ref=home.at[b],
            send_sem=home_sem.at[0, b],
            recv_sem=home_sem.at[1, b],
            device_id={"sp": partner},
            device_id_type=MESH,
        )
        copy.start()
        homes.append(copy)

    def store_own(lines, cols, value):
        hold[lines, cols] = mixed_ref[lines, cols] + value

    dispatch(0)
    dispatch(1)
    loads[0].wait()
    loads[1].wait()
    serve(0)
    relays[0].wait_recv()
    dispatch(2)
    serve(1)
    relays[1].wait_recv()
    dispatch(3)
    serve(2)
    serve(3)
    send_home(0)
    send_home(1)
    combine(0, store_own)
    combine(1, store_own)
    for b in range(2):
        homes[b].wait_recv()
        lines = slice(b * few, (b + 1) * few)
        out_ref[lines] = (hold[lines] + home[b].astype(F32)).astype(BF16)
    for b in range(2):
        relays[b].wait_send()
        homes[b].wait_send()
    for r in range(4):
        for k in range(1, half):
            go[r, k].wait_send()
            back[r, k].wait_send()


def layer_kernel(n, dp, capacity, *refs):
    inputs, refs = refs[:10], refs[10:]
    weights, out_ref, refs = refs[:3], refs[3], refs[4:]
    middle, refs = refs[:4], refs[4:]
    attention, refs = refs[:38], refs[38:]
    load_sem, stores, experts = refs[0], refs[1:4], refs[4:]
    loads = [
        pltpu.make_async_copy(src.at[0], dst, load_sem.at[i])
        for i, (src, dst) in enumerate(zip(weights, stores))
    ]

    def start_loads():
        for load in loads:
            load.start()

    attention_part(n, dp, start_loads, *inputs, *middle, *attention)
    mixed, normed, own, other = middle
    expert_part(n, capacity, normed, mixed, own, other, loads, out_ref, *stores, *experts)


def on_device(
    n,
    dp,
    queries,
    key_rows,
    values,
    query_gain,
    key_gain,
    out_weight,
    residual,
    norm_gain,
    expert_gate,
    expert_up,
    expert_down,
    routes,
    route_weight,
):
    _, rows, heads, width = queries.shape
    kv_heads = key_rows.shape[2]
    model = heads * width
    length = rows * n
    experts = expert_gate.shape[0] * n
    capacity = max(2, 4 * (rows // 2) // experts)
    slots = n // 2 * capacity
    across = max(x for x in range(1, n + 1) if n % x == 0 and x * x <= n)
    depth = n // across
    local_kv, local = kv_heads // across, heads // across
    units = across * local_kv
    w_rows, w_cols = out_weight.shape
    dma = pltpu.SemaphoreType.DMA
    ny = dp // 2
    ff = expert_gate.shape[2]
    few = rows // 2
    attention_scratch = [
        pltpu.VMEM((rows, heads, width), BF16),
        pltpu.VMEM((rows, kv_heads, width), BF16),
        pltpu.VMEM((rows, kv_heads, width), BF16),
        pltpu.VMEM((rows, heads, width), F32),
        pltpu.VMEM((across, 2 * local_kv, rows, width), BF16),
        pltpu.VMEM((across - 1, local, rows, width), BF16),
        pltpu.VMEM((local, across * rows, width), BF16),
        pltpu.VMEM((2 * local_kv, length, width), BF16),
        pltpu.VMEM((w_rows * n, w_cols), BF16),
        pltpu.VMEM((across - 1, rows, local * width), BF16),
        pltpu.VMEM((dp, rows, model), BF16),
        pltpu.VMEM((dp, rows, w_cols), BF16),
        pltpu.VMEM((dp, rows, w_cols), BF16),
        pltpu.VMEM((rows, model), BF16),
        pltpu.VMEM((2, 1, width), F32),
        pltpu.VMEM((1, model), F32),
        dma((8,)),
        dma((across, local_kv)),
        dma((across, local_kv)),
        dma((units, depth, 2)),
        dma((units, depth)),
        dma((across,)),
        dma((across,)),
        dma((4, depth, across)),
        dma((4, depth, across)),
        dma((4, depth, 2)),
        dma((4, depth)),
        dma((across, local_kv)),
        dma((across, local_kv)),
        dma((2,)),
        dma((ny, units)),
        dma((ny, units)),
        dma((units,)),
        dma((units,)),
        dma((ny, units)),
        dma((ny, units)),
        dma((dp, 2)),
        dma((dp, 2)),
    ]
    result = pl.pallas_call(
        functools.partial(layer_kernel, n, dp, capacity),
        out_shape=jax.ShapeDtypeStruct((rows, model), BF16),
        in_specs=[ANY] * 8 + [VMEM] * 2 + [ANY] * 3,
        out_specs=VMEM,
        scratch_shapes=[
            pltpu.VMEM((rows, model), F32),
            pltpu.VMEM((rows, model), BF16),
            pltpu.VMEM((rows, width), F32),
            pltpu.VMEM((rows, width), F32),
            *attention_scratch,
            dma((3,)),
            pltpu.VMEM((model, ff), BF16),
            pltpu.VMEM((model, ff), BF16),
            pltpu.VMEM((ff, model), BF16),
            pltpu.VMEM((2, few, model), BF16),
            pltpu.VMEM((4, slots, model), BF16),
            pltpu.VMEM((4, slots, model), BF16),
            pltpu.VMEM((slots, ff), BF16),
            pltpu.VMEM((4, slots, model), BF16),
            pltpu.VMEM((4, slots, model), BF16),
            pltpu.VMEM((rows, model), BF16),
            pltpu.VMEM((2, few, model), BF16),
            pltpu.VMEM((rows, model), F32),
            dma((2, 2)),
            dma((2, 2)),
            dma((4, n)),
            dma((4, n)),
            dma((4, n)),
            dma((4, n)),
        ],
        compiler_params=pltpu.CompilerParams(
            collective_id=0, has_side_effects=True, vmem_limit_bytes=56 * 1024 * 1024
        ),
        name="layer",
    )(
        queries[0],
        key_rows[0],
        values[0],
        query_gain[None],
        key_gain[None],
        out_weight,
        residual[0],
        norm_gain[None],
        routes[0].T,
        route_weight[0].T,
        expert_gate,
        expert_up,
        expert_down,
    )
    return result[None]


def solution(mesh):
    in_specs = (
        P("dp", "sp", None, None),
        P("dp", "sp", None, None),
        P("dp", "sp", None, None),
        P(),
        P(),
        P("sp", "dp"),
        P("dp", "sp", None),
        P(),
        P("sp", None, None),
        P("sp", None, None),
        P("sp", None, None),
        P("dp", "sp", None),
        P("dp", "sp", None),
    )
    out_specs = P("dp", "sp", None)
    return jax.shard_map(
        functools.partial(on_device, mesh.shape["sp"], mesh.shape["dp"]),
        mesh=mesh,
        in_specs=in_specs,
        out_specs=out_specs,
        check_vma=False,
    )
```

time: 164 us -> 144 us (0.88)
  the two profiles are of different devices: /device:TPU:8 before, /device:TPU:0 now
where the time goes in v1:
time: 144 us
  Pallas kernels  142 us (99%)
  local copies, waits for them, and re-layouts  1.88 us (1%)
    pallas_call x1, Pallas kernels, on_device(): pl.pallas_call(functools.partial(layer_kernel, n, dp, capacity), out_shap...  142 us

profile of v1, /device:TPU:0, one launch (start us, length us, event | category | flops | bytes accessed | tf_op | source)
XLA Modules:
  0.0 144.1 jit_solution(8320976021808315971)
XLA Ops:
  0.0 142.3 %layer.1 = bf16[128,2048]{1,0:T(8,128)(2,1)} custom-call(bf16[128,16,128]{2,1,0:T(8,128)(2,1)} %bitcast.15, bf16[128,4,128]{2,1,0:T(4,128)(2,1)} %bitcast.17, bf16[128,4,128]{2,1,0:T(4,128)(2,1)} %bitcast.18, f32[1,128]{1,0:T(1,128)} %bitcast.22, f32[1,128]{1,0:T(1,128)} %bitcast.23, bf16[256,512]{1,0:T(8,128)(2,1)} %refs_5_.1, bf16[128,2048]{1,0:T(8,128)(2,1)} %bitcast.16, ...), custom_call_target="tpu_custom_call" | custom-call | tf_op jit(solution)/shard_map/layer/pallas_call | solution.py:816
  142.3 1.9 %copy.15 = bf16[1,128,2048]{2,1,0:T(8,128)(2,1)} copy(bf16[1,128,2048]{2,1,0:T(8,128)(2,1)} %bitcast.14) | data formatting | bytes 1048576

commit v2 on v1

--- a/solution.py
+++ b/solution.py
@@ -10,6 +10,8 @@
 
 GRID_W = 64
 EPS = 1e-06
+CHUNKS = 4
+TILE = 256
 THETA = 10000.0
 MESH = pl.DeviceIdType.MESH
 VMEM = pl.BlockSpec(memory_space=pltpu.VMEM)
@@ -98,24 +100,30 @@
                 self.copy(unit, plane, way, target).wait_send()
 
 
-def slot_choice(table, base, slots, capacity):
-    rows = table.shape[0]
-    slot = lax.broadcasted_iota(jnp.int32, (rows, slots), 1)
-    expert = (slot // capacity + base).astype(F32)
-    first = table[:, 0:1] == expert
-    second = table[:, 1:2] == expert
+def selection(table, first_expert, column, columns, capacity):
+    rows = table.shape[1]
+    few = rows // 2
+    slots = columns * 2 * capacity
+    slot = lax.broadcasted_iota(jnp.int32, (slots, rows), 0)
+    row = lax.broadcasted_iota(jnp.int32, (slots, rows), 1)
+    side = (column + slot // (2 * capacity)) % columns
+    expert = (first_expert + side).astype(F32)
+    same = (slot // capacity) % 2 == row // few
+    first = (table[0:1, :] == expert) & same
+    second = (table[1:2, :] == expert) & same
     named = jnp.where(first | second, 1.0, 0.0).astype(BF16)
-    earlier = lax.broadcasted_iota(jnp.int32, (rows, rows), 1) < lax.broadcasted_iota(
-        jnp.int32, (rows, rows), 0
-    )
-    rank = jnp.dot(
-        jnp.where(earlier, 1.0, 0.0).astype(BF16), named, preferred_element_type=F32
-    )
+    before = lax.broadcasted_iota(jnp.int32, (rows, rows), 0)
+    after = lax.broadcasted_iota(jnp.int32, (rows, rows), 1)
+    earlier = jnp.where(before < after, 1.0, 0.0).astype(BF16)
+    rank = jnp.dot(named, earlier, preferred_element_type=F32)
     here = rank == (slot % capacity).astype(F32)
-    return (
-        jnp.where(first & here, 1.0, 0.0).astype(BF16),
-        jnp.where(second & here, 1.0, 0.0).astype(BF16),
-    )
+    choice = jnp.where((first | second) & here, 1.0, 0.0)
+    weight = jnp.where(first & here, table[2:3, :], 0.0)
+    weight = weight + jnp.where(second & here, table[3:4, :], 0.0)
+    weight = weight.T
+    high = weight.astype(BF16)
+    low = (weight - high.astype(F32)).astype(BF16)
+    return choice.astype(BF16), high, low
 
 
 def attention_part(
@@ -130,12 +138,9 @@
     w_ref,
     res_ref,
     ng_ref,
-    routes_ref,
-    gates_ref,
     mixed_ref,
     normed_ref,
-    own_table,
-    table,
+    prepare,
     q_in,
     k_in,
     v_in,
@@ -165,7 +170,6 @@
     wz_recv,
     ax_send,
     ax_recv,
-    t_sem,
     y_send,
     y_recv,
     pair_send,
@@ -350,19 +354,7 @@
             w_line.down(depth - 1 - z == t, u, z)
 
     w_begin(0)
-    lanes = jnp.concatenate(
-        [
-            routes_ref[...].astype(F32),
-            gates_ref[...],
-            jnp.zeros((width - 4, rows), F32),
-        ],
-        axis=0,
-    )
-    own_table[...] = lanes.T
-    table_copy = remote(
-        own_table, table, t_sem.at[0], t_sem.at[1], sp=lax.rem(me + n // 2, n)
-    )
-    table_copy.start()
+    prepare(0)
     for u in range(len(w_units)):
         w_across(always, u, z)
     for t in range(1, depth):
@@ -372,6 +364,7 @@
     middle = (z > 0) & (z < depth - 1)
     for u in range(len(w_units)):
         w_line.step(1, u, middle, w_across)
+    prepare(1)
     for k in range(1, across):
         remote(
             q_stage.at[0],
@@ -513,7 +506,6 @@
     for copies in (kvx, qx, ax):
         for copy in copies.values():
             copy.wait_send()
-    table_copy.wait()
     fetches[6].wait()
     fetches[7].wait()
     for copies in (y_copies, pair_copies, fwd_copies):
@@ -533,199 +525,436 @@
         normed_ref[:, cols] = (mixed_ref[:, cols] * factor * norm_in[:, cols]).astype(BF16)
 
 
-def expert_part(
-    n,
-    capacity,
-    normed_ref,
-    mixed_ref,
-    own_ref,
-    other_ref,
-    loads,
-    out_ref,
-    gate,
-    up,
-    down,
-    relay,
-    sent,
-    recv,
-    hidden,
-    res,
-    ret,
-    part,
-    home,
-    hold,
-    relay_sem,
-    home_sem,
-    go_send,
-    go_recv,
-    ret_send,
-    ret_recv,
-):
-    me = lax.axis_index("sp")
-    half = n // 2
-    base = me // half * half
-    mine = me % half
-    partner = lax.rem(me + half, n)
-    rows, model = normed_ref.shape
-    few = rows // 2
-    slots = half * capacity
-    ff = gate.shape[1]
-
-    def peer(k):
-        return base + lax.rem(mine + k, half)
-
-    relays = []
-    for b in range(2):
-        copy = pltpu.make_async_remote_copy(
-            src_ref=normed_ref.at[pl.ds(b * few, few)],
-            dst_ref=relay.at[b],
-            send_sem=relay_sem.at[0, b],
-            recv_sem=relay_sem.at[1, b],
-            device_id={"sp": partner},
+class Experts:
+    def __init__(self, n, capacity, routes, gates, middle, loads, out, *refs):
+        (
+            self.gate,
+            self.up,
+            self.down,
+            self.tables,
+            self.pick,
+            self.high,
+            self.low,
+            self.column,
+            self.asked,
+            self.served,
+            self.answer,
+            self.given,
+            self.acc,
+            self.hidden,
+            self.partial,
+            self.incoming,
+            self.hold,
+            self.result,
+            self.table_sem,
+            self.column_send,
+            self.column_recv,
+            self.ask_send,
+            self.ask_recv,
+            self.give_send,
+            self.give_recv,
+            self.part_send,
+            self.part_recv,
+            self.out_sem,
+        ) = refs
+        self.mixed, self.normed = middle
+        self.routes, self.gates = routes, gates
+        self.loads, self.out = loads, out
+        me = lax.axis_index("sp")
+        self.columns = max(x for x in range(1, n + 1) if n % x == 0 and x * x <= n)
+        self.depth = n // self.columns
+        self.z, self.x = me // self.columns, me % self.columns
+        self.upper = self.z // (self.depth // 2)
+        self.way = 1 - 2 * self.upper
+        self.inner = self.upper * (self.depth - 1) + self.way * self.z
+        self.capacity = capacity
+        self.rows, self.model = self.normed.shape
+        self.width = self.model // CHUNKS
+        self.share = 2 * capacity
+        self.started = []
+
+    def role(self, inner):
+        return self.inner == inner
+
+    def plane(self, r):
+        place = (self.inner, 1 - self.inner, self.depth - 1, self.depth - 2)[r]
+        return self.upper * (self.depth - 1) + self.way * place
+
+    def remote(self, src, dst, send, recv, target):
+        return pltpu.make_async_remote_copy(
+            src_ref=src,
+            dst_ref=dst,
+            send_sem=send,
+            recv_sem=recv,
+            device_id={"sp": target},
             device_id_type=MESH,
         )
-        copy.start()
-        relays.append(copy)
-
-    def block(index):
-        return pl.ds(pl.multiple_of(index * capacity, capacity), capacity)
-
-    go, back, homes = {}, {}, []
-
-    def choices(r):
-        table = own_ref if r < 2 else other_ref
-        return slot_choice(table[(r % 2) * few : (r % 2 + 1) * few], base, slots, capacity)
-
-    def dispatch(r):
-        first, second = choices(r)
-        choice = first + second
-        lines = normed_ref[(r % 2) * few : (r % 2 + 1) * few] if r < 2 else relay[r % 2]
-        for t in range(model // 512):
-            cols = slice(t * 512, (t + 1) * 512)
-            sent[r, :, cols] = lax.dot_general(
-                choice, lines[:, cols], (((0,), (0,)), ((), ())), preferred_element_type=F32
+
+    def at(self, step):
+        return (self.z + step) * self.columns + self.x
+
+    def beside(self, k):
+        return self.z * self.columns + (self.x + k) % self.columns
+
+    def cols(self, c):
+        return slice(c * self.width, (c + 1) * self.width)
+
+    def send(self, make, inner=None):
+        if inner is None:
+            make().start()
+        else:
+
+            @pl.when(self.role(inner))
+            def _():
+                make().start()
+
+        self.started.append((make, inner))
+
+    def prepare(self, phase):
+        planes = self.depth
+
+        def table_copy(d):
+            target = (self.z + d) % planes
+            return self.remote(
+                self.tables.at[self.z],
+                self.tables.at[self.z],
+                self.table_sem.at[0, d],
+                self.table_sem.at[1, d],
+                target * self.columns + self.x,
+            )
+
+        if phase == 0:
+            rows = self.rows
+            self.tables[self.z] = jnp.concatenate(
+                [self.routes[...].astype(F32), self.gates[...], jnp.zeros((4, rows), F32)], axis=0
+            )
+            for d in range(1, planes):
+                self.send(functools.partial(table_copy, d))
+            return
+        for d in range(1, planes):
+            table_copy(d).wait_recv()
+        for r in range(planes):
+            choice, high, low = selection(
+                self.tables[self.plane(r)],
+                self.z * self.columns,
+                self.x,
+                self.columns,
+                self.capacity,
+            )
+            self.pick[r] = choice
+            self.high[r] = high
+            self.low[r] = low
+
+    def column_copy(self, kind, c):
+        source, place, step = {
+            "forth": (None, None, 1),
+            "back": (None, 1, -1),
+            1: (1, 2, 1),
+            2: (2, 2, -1),
+            3: (3, 3, -1),
+        }[kind]
+        cols = self.cols(c)
+        src = self.normed.at[:, cols] if source is None else self.column.at[source - 1, :, cols]
+        if place is None:
+            place = 1 + 2 * self.inner
+        index = ("forth", "back", 1, 2, 3).index(kind)
+        return self.remote(
+            src,
+            self.column.at[place - 1, :, cols],
+            self.column_send.at[index, c],
+            self.column_recv.at[place - 1, c],
+            self.at(step * self.way),
+        )
+
+    def column_arrive(self, r, c):
+        cols = self.cols(c)
+        self.remote(
+            self.column.at[r - 1, :, cols],
+            self.column.at[r - 1, :, cols],
+            self.column_send.at[0, c],
+            self.column_recv.at[r - 1, c],
+            self.at(0),
+        ).wait_recv()
+
+    def ask_copy(self, r, c, k):
+        cols = self.cols(c)
+        return self.remote(
+            self.asked.at[r, pl.ds((k - 1) * self.share, self.share), cols],
+            self.served.at[r, pl.ds((self.columns - k) * self.share, self.share), cols],
+            self.ask_send.at[r, c, k],
+            self.ask_recv.at[r, c, self.columns - k],
+            self.beside(k),
+        )
+
+    def give_copy(self, r, c, k):
+        cols = self.cols(c)
+        return self.remote(
+            self.given.at[r, pl.ds((k - 1) * self.share, self.share), cols],
+            self.answer.at[r, pl.ds((self.columns - k) * self.share, self.share), cols],
+            self.give_send.at[r, c, k],
+            self.give_recv.at[r, c, self.columns - k],
+            self.beside(k),
+        )
+
+    def ask(self, r, c, inner=None):
+        def body():
+            cols = self.cols(c)
+            if r > 0:
+                self.column_arrive(r, c)
+            if r > 0 and inner != 0:
+
+                @pl.when(self.role(1))
+                def _():
+                    self.column_copy(r, c).start()
+
+            lines = self.normed[:, cols] if r == 0 else self.column[r - 1, :, cols]
+            chosen = jnp.dot(self.pick[r], lines, preferred_element_type=F32).astype(BF16)
+            self.served[r, 0 : self.share, cols] = chosen[0 : self.share]
+            for k in range(1, self.columns):
+                part = slice((k - 1) * self.share, k * self.share)
+                self.asked[r, part, cols] = chosen[k * self.share : (k + 1) * self.share]
+                self.ask_copy(r, c, k).start()
+
+        if inner is None:
+            body()
+        else:
+            pl.when(self.role(inner))(body)
+
+    def serve_up(self, r, h):
+        for c in range(h * CHUNKS // 2, (h + 1) * CHUNKS // 2):
+            for k in range(1, self.columns):
+                self.ask_copy(r, c, self.columns - k).wait_recv()
+        if r == 0 and h == 0:
+            self.loads[0].wait()
+            self.loads[1].wait()
+        deep = slice(h * self.model // 2, (h + 1) * self.model // 2)
+        acc = self.acc
+
+        def up_tile(t, carry):
+            cols = pl.ds(pl.multiple_of(t * TILE, TILE), TILE)
+            lines = self.served[r, :, deep]
+            gate = jnp.dot(lines, self.gate[deep, cols], preferred_element_type=F32)
+            up = jnp.dot(lines, self.up[deep, cols], preferred_element_type=F32)
+            if h == 0:
+                acc[0, :, cols] = gate
+                acc[1, :, cols] = up
+            else:
+                gate = gate + acc[0, :, cols]
+                up = up + acc[1, :, cols]
+                self.hidden[:, cols] = (gate / (1.0 + jnp.exp(-gate)) * up).astype(BF16)
+            return carry
+
+        lax.fori_loop(0, self.gate.shape[1] // TILE, up_tile, 0)
+
+    def serve_down(self, r, c):
+        if r == 0 and c == 0:
+            self.loads[2].wait()
+
+        def down_tile(t, carry):
+            cols = pl.ds(pl.multiple_of(c * self.width + t * TILE, TILE), TILE)
+            lines = jnp.dot(
+                self.hidden[...], self.down[:, cols], preferred_element_type=F32
             ).astype(BF16)
-        recv[r, block(mine)] = sent[r, block(mine)]
-        for k in range(1, half):
-            copy = pltpu.make_async_remote_copy(
-                src_ref=sent.at[r, block(lax.rem(mine + k, half))],
-                dst_ref=recv.at[r, block(mine)],
-                send_sem=go_send.at[r, k],
-                recv_sem=go_recv.at[r, k],
-                device_id={"sp": peer(k)},
-                device_id_type=MESH,
-            )
-            copy.start()
-            go[r, k] = copy
-
-    tile = 256
-
-    def serve(r):
-        for k in range(1, half):
-            go[r, k].wait_recv()
-
-        def up_tile(t, carry):
-            cols = pl.ds(pl.multiple_of(t * tile, tile), tile)
-            gate_part = jnp.dot(recv[r], gate[:, cols], preferred_element_type=F32)
-            up_part = jnp.dot(recv[r], up[:, cols], preferred_element_type=F32)
-            hidden[:, cols] = (gate_part / (1.0 + jnp.exp(-gate_part)) * up_part).astype(BF16)
+            self.answer[r, 0 : self.share, cols] = lines[0 : self.share]
+            self.given[r, :, cols] = lines[self.share :]
             return carry
 
-        lax.fori_loop(0, ff // tile, up_tile, 0)
-        if r == 0:
-            loads[2].wait()
-
-        def down_tile(t, carry):
-            cols = pl.ds(pl.multiple_of(t * tile, tile), tile)
-            res[r, :, cols] = jnp.dot(
-                hidden[...], down[:, cols], preferred_element_type=F32
-            ).astype(BF16)
-            return carry
-
-        lax.fori_loop(0, model // tile, down_tile, 0)
-        ret[r, block(mine)] = res[r, block(mine)]
-        for k in range(1, half):
-            copy = pltpu.make_async_remote_copy(
-                src_ref=res.at[r, block(lax.rem(mine + k, half))],
-                dst_ref=ret.at[r, block(mine)],
-                send_sem=ret_send.at[r, k],
-                recv_sem=ret_recv.at[r, k],
-                device_id={"sp": peer(k)},
-                device_id_type=MESH,
-            )
-            copy.start()
-            back[r, k] = copy
-
-    def combine(r, store):
-        first, second = choices(r)
-        table = own_ref if r < 2 else other_ref
-        lines = slice((r % 2) * few, (r % 2 + 1) * few)
-        for k in range(1, half):
-            back[r, k].wait_recv()
-        for t in range(model // 512):
-            cols = slice(t * 512, (t + 1) * 512)
-            served = ret[r, :, cols]
-            store(
-                lines,
-                cols,
-                jnp.dot(first, served, preferred_element_type=F32) * table[lines, 2:3]
-                + jnp.dot(second, served, preferred_element_type=F32) * table[lines, 3:4],
-            )
-
-    def store_part(lines, cols, value):
-        part[lines, cols] = value.astype(BF16)
-
-    def send_home(b):
-        combine(2 + b, store_part)
-        copy = pltpu.make_async_remote_copy(
-            src_ref=part.at[pl.ds(b * few, few)],
-            dst_ref=home.at[b],
-            send_sem=home_sem.at[0, b],
-            recv_sem=home_sem.at[1, b],
-            device_id={"sp": partner},
-            device_id_type=MESH,
+        lax.fori_loop(0, self.width // TILE, down_tile, 0)
+        for k in range(1, self.columns):
+            self.give_copy(r, c, k).start()
+
+    def combine(self, r, c):
+        for k in range(1, self.columns):
+            self.give_copy(r, c, self.columns - k).wait_recv()
+        lines = self.answer[r, :, self.cols(c)]
+        return jnp.dot(self.high[r], lines, preferred_element_type=F32) + jnp.dot(
+            self.low[r], lines, preferred_element_type=F32
         )
-        copy.start()
-        homes.append(copy)
-
-    def store_own(lines, cols, value):
-        hold[lines, cols] = mixed_ref[lines, cols] + value
-
-    dispatch(0)
-    dispatch(1)
-    loads[0].wait()
-    loads[1].wait()
-    serve(0)
-    relays[0].wait_recv()
-    dispatch(2)
-    serve(1)
-    relays[1].wait_recv()
-    dispatch(3)
-    serve(2)
-    serve(3)
-    send_home(0)
-    send_home(1)
-    combine(0, store_own)
-    combine(1, store_own)
-    for b in range(2):
-        homes[b].wait_recv()
-        lines = slice(b * few, (b + 1) * few)
-        out_ref[lines] = (hold[lines] + home[b].astype(F32)).astype(BF16)
-    for b in range(2):
-        relays[b].wait_send()
-        homes[b].wait_send()
-    for r in range(4):
-        for k in range(1, half):
-            go[r, k].wait_send()
-            back[r, k].wait_send()
+
+    def part_copy(self, slot, place, step, c):
+        cols = self.cols(c)
+        return self.remote(
+            self.partial.at[slot, :, cols],
+            self.incoming.at[place, :, cols],
+            self.part_send.at[slot, c],
+            self.part_recv.at[place, c],
+            self.at(step * self.way),
+        )
+
+    def part_arrive(self, place, c):
+        cols = self.cols(c)
+        self.remote(
+            self.partial.at[0, :, cols],
+            self.incoming.at[place, :, cols],
+            self.part_send.at[0, c],
+            self.part_recv.at[place, c],
+            self.at(0),
+        ).wait_recv()
+        return self.incoming[place, :, cols].astype(F32)
+
+    def merge(self, inner, r, c, slot, place, step, feed=None):
+        @pl.when(self.role(inner))
+        def _():
+            total = self.combine(r, c)
+            if feed is not None:
+                total = total + self.part_arrive(feed, c)
+            self.partial[slot, :, self.cols(c)] = total.astype(BF16)
+            self.part_copy(slot, place, step, c).start()
+
+    def own(self, c):
+        cols = self.cols(c)
+        self.hold[:, cols] = self.mixed[:, cols] + self.combine(0, c)
+
+    def finish(self, inner, places):
+        @pl.when(self.role(inner))
+        def _():
+            for c in range(CHUNKS):
+                cols = self.cols(c)
+                total = self.hold[:, cols]
+                for place in places:
+                    total = total + self.part_arrive(place, c)
+                self.result[:, cols] = total.astype(BF16)
+                self.out_copy(c).start()
+
+    def out_copy(self, c):
+        cols = self.cols(c)
+        return pltpu.make_async_copy(
+            self.result.at[:, cols], self.out.at[:, cols], self.out_sem.at[c]
+        )
+
+    def run(self):
+        chunks = range(CHUNKS)
+        half = CHUNKS // 2
+
+        def forth(cs):
+            for c in cs:
+                self.column_copy("forth", c).start()
+
+        for c in chunks:
+
+            @pl.when(self.role(1))
+            def _():
+                self.column_copy("back", c).start()
+
+            if c < half:
+                self.column_copy("forth", c).start()
+            else:
+
+                @pl.when(self.role(0))
+                def _():
+                    self.column_copy("forth", c).start()
+
+        for c in chunks:
+            self.ask(0, c)
+        self.ask(1, 0)
+        self.serve_up(0, 0)
+        self.ask(1, 1)
+        self.serve_up(0, 1)
+        self.ask(1, 2)
+        self.ask(2, 0, 1)
+        self.serve_up(1, 0)
+        self.ask(1, 3)
+
+        @pl.when(self.role(1))
+        def _():
+            forth(range(half, CHUNKS))
+
+        self.ask(2, 1, 1)
+        for c in chunks:
+            self.serve_down(0, c)
+        self.ask(2, 0, 0)
+        self.ask(2, 2, 1)
+        self.serve_up(1, 1)
+        self.serve_down(1, 0)
+        self.serve_down(1, 1)
+        self.ask(2, 1, 0)
+        self.ask(2, 3, 1)
+        self.serve_down(1, 2)
+        self.serve_down(1, 3)
+        self.ask(3, 0, 1)
+        self.ask(3, 1, 1)
+        self.ask(2, 2, 0)
+        self.merge(0, 1, 0, 0, 0, 1)
+        self.merge(0, 1, 1, 0, 0, 1)
+        self.serve_up(2, 0)
+        self.ask(2, 3, 0)
+        self.ask(3, 2, 1)
+        self.merge(0, 1, 2, 0, 0, 1)
+        self.merge(0, 1, 3, 0, 0, 1)
+        self.ask(3, 0, 0)
+        self.ask(3, 3, 1)
+        self.serve_up(2, 1)
+        self.serve_down(2, 0)
+        self.serve_down(2, 1)
+        self.ask(3, 1, 0)
+        self.serve_down(2, 2)
+        self.serve_down(2, 3)
+        self.ask(3, 2, 0)
+        self.merge(0, 2, 0, 1, 1, 1)
+        self.merge(0, 2, 1, 1, 1, 1)
+        self.serve_up(3, 0)
+        self.ask(3, 3, 0)
+        self.merge(0, 2, 2, 1, 1, 1)
+        self.merge(0, 2, 3, 1, 1, 1)
+        self.own(0)
+        self.own(1)
+        self.serve_up(3, 1)
+        for c in chunks:
+            self.serve_down(3, c)
+        for c in chunks:
+            self.merge(0, 3, c, 2, 2, 1)
+        self.own(2)
+        self.own(3)
+
+        def far(c):
+            self.merge(1, 2, c, 1, 3, 1, 1)
+
+        def near(c):
+            self.merge(1, 1, c, 3, 5, -1, 3)
+
+        for c in chunks:
+            far(c)
+            if c > 0:
+                near(c - 1)
+        near(CHUNKS - 1)
+        for c in chunks:
+            self.merge(1, 3, c, 2, 4, 1, 2)
+        self.finish(0, (5,))
+        self.finish(1, (0, 4))
+        self.drain()
+
+    def drain(self):
+        for make, _ in self.started:
+            make().wait_send()
+        for c in range(CHUNKS):
+            self.column_copy("forth", c).wait_send()
+
+            @pl.when(self.role(1))
+            def _():
+                self.column_copy("back", c).wait_send()
+                for r in (1, 2, 3):
+                    self.column_copy(r, c).wait_send()
+                for slot, place, step in ((1, 3, 1), (2, 4, 1), (3, 5, -1)):
+                    self.part_copy(slot, place, step, c).wait_send()
+
+            @pl.when(self.role(0))
+            def _():
+                for slot in range(3):
+                    self.part_copy(slot, slot, 1, c).wait_send()
+
+            for r in range(self.depth):
+                for k in range(1, self.columns):
+                    self.ask_copy(r, c, k).wait_send()
+                    self.give_copy(r, c, k).wait_send()
+            self.out_copy(c).wait()
 
 
 def layer_kernel(n, dp, capacity, *refs):
     inputs, refs = refs[:10], refs[10:]
     weights, out_ref, refs = refs[:3], refs[3], refs[4:]
-    middle, refs = refs[:4], refs[4:]
-    attention, refs = refs[:38], refs[38:]
-    load_sem, stores, experts = refs[0], refs[1:4], refs[4:]
+    middle, refs = refs[:2], refs[2:]
+    attention, refs = refs[:37], refs[37:]
+    load_sem, stores = refs[0], refs[1:4]
     loads = [
         pltpu.make_async_copy(src.at[0], dst, load_sem.at[i])
         for i, (src, dst) in enumerate(zip(weights, stores))
@@ -735,9 +964,9 @@
         for load in loads:
             load.start()
 
-    attention_part(n, dp, start_loads, *inputs, *middle, *attention)
-    mixed, normed, own, other = middle
-    expert_part(n, capacity, normed, mixed, own, other, loads, out_ref, *stores, *experts)
+    experts = Experts(n, capacity, *inputs[8:], middle, loads, out_ref, *refs[1:])
+    attention_part(n, dp, start_loads, *inputs[:8], *middle, experts.prepare, *attention)
+    experts.run()
 
 
 def on_device(
@@ -763,16 +992,16 @@
     length = rows * n
     experts = expert_gate.shape[0] * n
     capacity = max(2, 4 * (rows // 2) // experts)
-    slots = n // 2 * capacity
     across = max(x for x in range(1, n + 1) if n % x == 0 and x * x <= n)
     depth = n // across
     local_kv, local = kv_heads // across, heads // across
     units = across * local_kv
+    slots = 2 * across * capacity
+    aside = 2 * (across - 1) * capacity
     w_rows, w_cols = out_weight.shape
     dma = pltpu.SemaphoreType.DMA
     ny = dp // 2
     ff = expert_gate.shape[2]
-    few = rows // 2
     attention_scratch = [
         pltpu.VMEM((rows, heads, width), BF16),
         pltpu.VMEM((rows, kv_heads, width), BF16),
@@ -803,7 +1032,6 @@
         dma((4, depth)),
         dma((across, local_kv)),
         dma((across, local_kv)),
-        dma((2,)),
         dma((ny, units)),
         dma((ny, units)),
         dma((units,)),
@@ -817,32 +1045,40 @@
         functools.partial(layer_kernel, n, dp, capacity),
         out_shape=jax.ShapeDtypeStruct((rows, model), BF16),
         in_specs=[ANY] * 8 + [VMEM] * 2 + [ANY] * 3,
-        out_specs=VMEM,
+        out_specs=ANY,
         scratch_shapes=[
             pltpu.VMEM((rows, model), F32),
             pltpu.VMEM((rows, model), BF16),
-            pltpu.VMEM((rows, width), F32),
-            pltpu.VMEM((rows, width), F32),
             *attention_scratch,
             dma((3,)),
             pltpu.VMEM((model, ff), BF16),
             pltpu.VMEM((model, ff), BF16),
             pltpu.VMEM((ff, model), BF16),
-            pltpu.VMEM((2, few, model), BF16),
-            pltpu.VMEM((4, slots, model), BF16),
-            pltpu.VMEM((4, slots, model), BF16),
+            pltpu.VMEM((depth, 8, rows), F32),
+            pltpu.VMEM((depth, slots, rows), BF16),
+            pltpu.VMEM((depth, rows, slots), BF16),
+            pltpu.VMEM((depth, rows, slots), BF16),
+            pltpu.VMEM((depth - 1, rows, model), BF16),
+            pltpu.VMEM((depth, aside, model), BF16),
+            pltpu.VMEM((depth, slots, model), BF16),
+            pltpu.VMEM((depth, slots, model), BF16),
+            pltpu.VMEM((depth, aside, model), BF16),
+            pltpu.VMEM((2, slots, ff), F32),
             pltpu.VMEM((slots, ff), BF16),
-            pltpu.VMEM((4, slots, model), BF16),
-            pltpu.VMEM((4, slots, model), BF16),
+            pltpu.VMEM((4, rows, model), BF16),
+            pltpu.VMEM((6, rows, model), BF16),
+            pltpu.VMEM((rows, model), F32),
             pltpu.VMEM((rows, model), BF16),
-            pltpu.VMEM((2, few, model), BF16),
-            pltpu.VMEM((rows, model), F32),
-            dma((2, 2)),
-            dma((2, 2)),
-            dma((4, n)),
-            dma((4, n)),
-            dma((4, n)),
-            dma((4, n)),
+            dma((2, depth)),
+            dma((5, CHUNKS)),
+            dma((depth - 1, CHUNKS)),
+            dma((depth, CHUNKS, across)),
+            dma((depth, CHUNKS, across)),
+            dma((depth, CHUNKS, across)),
+            dma((depth, CHUNKS, across)),
+            dma((4, CHUNKS)),
+            dma((6, CHUNKS)),
+            dma((CHUNKS,)),
         ],
         compiler_params=pltpu.CompilerParams(
             collective_id=0, has_side_effects=True, vmem_limit_bytes=56 * 1024 * 1024

time: 144 us -> 133 us (0.924)
  the two profiles are of different devices: /device:TPU:0 before, /device:TPU:8 now
where the time goes in v2:
time: 133 us; the launch traced here: 131 us
  Pallas kernels  130 us (98%)
  local copies, waits for them, and re-layouts  1.88 us (1%)
    pallas_call x1, Pallas kernels, on_device(): pl.pallas_call(functools.partial(layer_kernel, n, dp, capacity), out_shap...  130 us

profile of v2, /device:TPU:8, one launch (start us, length us, event | category | flops | bytes accessed | tf_op | source)
XLA Modules:
  0.0 131.5 jit_solution(11011222074433364667)
XLA Ops:
  0.0 129.6 %layer.1 = bf16[128,2048]{1,0:T(8,128)(2,1)} custom-call(bf16[128,16,128]{2,1,0:T(8,128)(2,1)} %bitcast.15, bf16[128,4,128]{2,1,0:T(4,128)(2,1)} %bitcast.17, bf16[128,4,128]{2,1,0:T(4,128)(2,1)} %bitcast.18, f32[1,128]{1,0:T(1,128)} %bitcast.22, f32[1,128]{1,0:T(1,128)} %bitcast.23, bf16[256,512]{1,0:T(8,128)(2,1)} %refs_5_.1, bf16[128,2048]{1,0:T(8,128)(2,1)} %bitcast.16, ...), custom_call_target="tpu_custom_call" | custom-call | tf_op jit(solution)/shard_map/layer/pallas_call | solution.py:1044
  129.6 1.9 %copy.15 = bf16[1,128,2048]{2,1,0:T(8,128)(2,1)} copy(bf16[1,128,2048]{2,1,0:T(8,128)(2,1)} %bitcast.14) | data formatting | bytes 1048576

commit v3 on v2

--- a/solution.py
+++ b/solution.py
@@ -50,13 +50,12 @@
         self.send, self.recv = send, recv
         me = lax.axis_index("sp")
         self.z, self.x = me // width, me % width
-        self.ends = []
 
     def copy(self, unit, plane, way, target):
         return pltpu.make_async_remote_copy(
             src_ref=self.block(unit, plane * self.width + self.x),
             dst_ref=self.block(unit, plane * self.width + self.x),
-            send_sem=self.send.at[unit, plane, way],
+            send_sem=self.send.at[way],
             recv_sem=self.recv.at[unit, plane],
             device_id={"sp": target * self.width + self.x},
             device_id_type=MESH,
@@ -66,8 +65,6 @@
         @pl.when(condition)
         def _():
             self.copy(unit, plane, way, target).start()
-
-        self.ends.append((condition, unit, plane, way, target))
 
     def up(self, condition, unit, plane):
         self.start(condition & (self.z < self.depth - 1), unit, plane, 0, self.z + 1)
@@ -92,12 +89,21 @@
         if then is not None:
             then(above, unit, self.z + t)
 
-    def drain(self):
-        for condition, unit, plane, way, target in self.ends:
-
-            @pl.when(condition)
-            def _():
-                self.copy(unit, plane, way, target).wait_send()
+    def drain(self, planes):
+        for way in range(2):
+            for count in range(1, self.depth):
+                z = count - 1 if way == 0 else self.depth - count
+
+                @pl.when(self.z == z)
+                def _():
+                    pltpu.make_async_remote_copy(
+                        src_ref=planes(count),
+                        dst_ref=planes(count),
+                        send_sem=self.send.at[way],
+                        recv_sem=self.recv.at[0, 0],
+                        device_id={"sp": self.z * self.width + self.x},
+                        device_id_type=MESH,
+                    ).wait_send()
 
 
 def selection(table, first_expert, column, columns, capacity):
@@ -172,12 +178,9 @@
     ax_recv,
     y_send,
     y_recv,
-    pair_send,
-    pair_recv,
-    fwd_send,
-    fwd_recv,
-    back_send,
-    back_recv,
+    pair_sem,
+    fwd_sem,
+    back_sem,
 ):
     me = lax.axis_index("sp")
     mine = lax.axis_index("dp")
@@ -259,7 +262,8 @@
     def kv_block(g, sp):
         return kv.at[pl.ds(2 * g, 2), span(sp, rows), :]
 
-    kv_units = [(k, g) for k in range(across) for g in range(local_kv)]
+    kv_units = [(k, g) for g in range(local_kv) for k in range(across)]
+    own_units = [u for u, (k, _) in enumerate(kv_units) if k == 0]
 
     def kv_unit(u, sp):
         k, g = kv_units[u]
@@ -276,19 +280,19 @@
 
     kv_line = Line(depth, across, kv_unit, kvz_send, kvz_recv)
     w_line = Line(depth, across, w_unit, wz_send, wz_recv)
-    kvx, qx, ax, wx = {}, {}, {}, []
+    kvx, qx, ax = {}, {}, {}
     for g in range(local_kv):
         for k in range(1, across):
             kvx[k, g] = remote(
                 stage.at[lax.rem(x + k, across), pl.ds(2 * g, 2)],
                 kv_block(g, me),
-                kvx_send.at[k, g],
-                kvx_recv.at[across - k, g],
+                kvx_send.at[0],
+                kvx_recv.at[across - k - 1, g],
                 sp=beside(k),
             )
             kvx[k, g].start()
-        kv_line.up(always, g, z)
-        kv_line.down(always, g, z)
+        kv_line.up(always, own_units[g], z)
+        kv_line.down(always, own_units[g], z)
 
     start_loads()
     fetches[3].wait()
@@ -311,19 +315,20 @@
             qx[k] = remote(
                 q_stage.at[k - 1],
                 q_all.at[:, pl.ds((across - k) * rows, rows), :],
-                qx_send.at[k],
-                qx_recv.at[across - k],
+                qx_send.at[0],
+                qx_recv.at[0],
                 sp=beside(k),
             )
             qx[k].start()
         if k == across - 1:
-            for u in range(local_kv, len(kv_units)):
-                kk, g = kv_units[u]
+            for u, (kk, g) in enumerate(kv_units):
+                if kk == 0:
+                    continue
                 remote(
                     stage.at[0, pl.ds(2 * g, 2)],
                     kv_block(g, beside(kk)),
-                    kvx_send.at[kk, g],
-                    kvx_recv.at[kk, g],
+                    kvx_send.at[0],
+                    kvx_recv.at[kk - 1, g],
                     sp=me,
                 ).wait_recv()
                 kv_line.up(always, u, z)
@@ -333,20 +338,15 @@
     def w_across(condition, u, plane):
         for k in range(1, across):
 
-            def copy():
-                return remote(
+            @pl.when(condition)
+            def _():
+                remote(
                     w_unit(u, plane * across + x),
                     w_unit(u, plane * across + x),
-                    wx_send.at[u, plane, k],
-                    wx_recv.at[u, plane, across - k],
+                    wx_send.at[0],
+                    wx_recv.at[w_units[u][0]],
                     sp=beside(k),
-                )
-
-            @pl.when(condition)
-            def _():
-                copy().start()
-
-            wx.append((condition, copy))
+                ).start()
 
     def w_begin(t):
         for u in range(len(w_units)):
@@ -357,22 +357,19 @@
     prepare(0)
     for u in range(len(w_units)):
         w_across(always, u, z)
-    for t in range(1, depth):
+    for t in range(1, depth - 1):
         for u in range(len(kv_units)):
             kv_line.step(t, u)
         w_begin(t)
     middle = (z > 0) & (z < depth - 1)
-    for u in range(len(w_units)):
-        w_line.step(1, u, middle, w_across)
     prepare(1)
-    for k in range(1, across):
-        remote(
-            q_stage.at[0],
-            q_all.at[:, pl.ds(k * rows, rows), :],
-            qx_send.at[k],
-            qx_recv.at[k],
-            sp=me,
-        ).wait_recv()
+    remote(
+        q_stage,
+        q_all.at[:, pl.ds(rows, (across - 1) * rows), :],
+        qx_send.at[0],
+        qx_recv.at[0],
+        sp=me,
+    ).wait_recv()
 
     scale = width ** (-0.5)
     wide_group = group * width
@@ -381,31 +378,35 @@
         side = lax.rem(x + k, across)
         start = (side * local_kv + g) * wide_group
         return pl.ds(pl.multiple_of(start, wide_group), wide_group)
-
-    y_copies, pair_copies, fwd_copies = {}, {}, {}
 
     def spread_att(u):
         k, g = kv_units[u]
         block = att.at[mine, :, att_cols(k, g)]
         for j in range(1, ny):
             target = lax.rem(row_y + j, ny) * 2 + core
-            copy = remote(block, block, y_send.at[j, u], y_recv.at[j, u], dp=target)
-            copy.start()
-            y_copies[j, u] = copy
-        copy = remote(block, block, pair_send.at[u], pair_recv.at[u], dp=partner)
-        copy.start()
-        pair_copies[u] = copy
+            remote(block, block, y_send.at[0], y_recv.at[j - 1, u], dp=target).start()
+        remote(block, block, pair_sem.at[0], pair_sem.at[1], dp=partner).start()
 
     def forward(u):
         for j in range(1, ny):
             source = lax.rem(row_y + ny - j, ny) * 2 + core
-            y_copies[j, u].wait_recv()
+            remote(
+                att.at[mine, :, att_cols(*kv_units[u])],
+                att.at[mine, :, att_cols(*kv_units[u])],
+                y_send.at[0],
+                y_recv.at[j - 1, u],
+                dp=mine,
+            ).wait_recv()
             block = att.at[source, :, att_cols(*kv_units[u])]
-            copy = remote(block, block, fwd_send.at[j, u], fwd_recv.at[j, u], dp=partner)
-            copy.start()
-            fwd_copies[j, u] = copy
+            remote(block, block, fwd_sem.at[0], fwd_sem.at[1], dp=partner).start()
 
     for g in range(local_kv):
+        for u, (_, gg) in enumerate(kv_units):
+            if gg == g:
+                kv_line.step(depth - 1, u)
+        if g == local_kv - 1:
+            for u in range(len(w_units)):
+                w_line.step(1, u, middle, w_across)
 
         def one_head(i, carry):
             h = g * group + i
@@ -430,52 +431,51 @@
             ax[k, g] = remote(
                 swap.at[k - 1, :, pl.ds(g * wide_group, wide_group)],
                 att.at[mine, :, att_cols(0, g)],
-                ax_send.at[k, g],
-                ax_recv.at[across - k, g],
+                ax_send.at[0],
+                ax_recv.at[across - k - 1, g],
                 sp=beside(k),
             )
             ax[k, g].start()
-        spread_att(g)
-        if g == 0:
-            for u in range(len(w_units)):
-                w_line.step(1, u, jnp.logical_not(middle), w_across)
+        spread_att(own_units[g])
     for t in range(2, depth - 1):
         for u in range(len(w_units)):
-            w_line.step(t, u, True, w_across)
-    for u in range(local_kv, len(kv_units)):
-        k, g = kv_units[u]
+            w_line.step(t, u, middle, w_across)
+    for u in range(len(w_units)):
+        w_line.step(1, u, jnp.logical_not(middle), w_across)
+    for u, (k, g) in enumerate(kv_units):
+        if k == 0:
+            continue
         remote(
             swap.at[0, :, pl.ds(g * wide_group, wide_group)],
             att.at[mine, :, att_cols(k, g)],
-            ax_send.at[k, g],
-            ax_recv.at[k, g],
+            ax_send.at[0],
+            ax_recv.at[k - 1, g],
             sp=me,
         ).wait_recv()
         spread_att(u)
-    for u in range(len(kv_units)):
-        forward(u)
-    for u in range(len(w_units)):
-        w_line.step(depth - 1, u, True, w_across)
-    for u in range(len(kv_units)):
-        pair_copies[u].wait_recv()
-        for j in range(1, ny):
-            fwd_copies[j, u].wait_recv()
-
-    back_copies = {}
+    for t in range(2, depth - 1):
+        for u in range(len(w_units)):
+            w_line.step(t, u, jnp.logical_not(middle), w_across)
+    order = own_units + [u for u in range(len(kv_units)) if u not in own_units]
+    for i in range(max(len(order), len(w_units))):
+        if i < len(w_units):
+            w_line.step(depth - 1, i, True, w_across)
+        if i < len(order):
+            forward(order[i])
+    if ny > 1:
+        remote(
+            att.at[pl.ds(0, ny - 1)],
+            att.at[pl.ds(0, ny - 1)],
+            fwd_sem.at[0],
+            fwd_sem.at[1],
+            dp=mine,
+        ).wait_recv()
+    remote(att.at[mine], att.at[mine], pair_sem.at[0], pair_sem.at[1], dp=mine).wait_recv()
+
     for j in range(halves):
-        for u, (jj, _) in enumerate(w_units):
-            if jj != j:
-                continue
-            for plane in range(depth):
-                for k in range(1, across):
-                    remote(
-                        w_unit(u, plane * across + x),
-                        w_unit(u, plane * across + lax.rem(x + k, across)),
-                        wx_send.at[u, plane, k],
-                        wx_recv.at[u, plane, k],
-                        sp=me,
-                    ).wait_recv()
         cols = slice(j * part_cols, (j + 1) * part_cols)
+        block = w_full.at[pl.ds(0, depth * (across - 1) * w_rows), cols]
+        remote(block, block, wx_send.at[0], wx_recv.at[j], sp=me).wait_recv()
         result = jnp.dot(
             att[...].reshape(dp * rows, model), w_full[:, cols], preferred_element_type=F32
         ).astype(BF16)
@@ -485,34 +485,18 @@
         order = sorted(range(1, dp), key=lambda d: d % 2)
         for d in order:
             target = lax.rem(mine + d, dp)
-            copy = remote(
+            remote(
                 proj.at[target, :, cols],
                 back.at[mine, :, cols],
-                back_send.at[d, j],
-                back_recv.at[d, j],
+                back_sem.at[0],
+                back_sem.at[1],
                 dp=target,
-            )
-            copy.start()
-            back_copies[d, j] = copy
-
-    kv_line.drain()
-    w_line.drain()
-    for condition, copy in wx:
-
-        @pl.when(condition)
-        def _():
-            copy().wait_send()
-
-    for copies in (kvx, qx, ax):
-        for copy in copies.values():
-            copy.wait_send()
+            ).start()
+
     fetches[6].wait()
     fetches[7].wait()
-    for copies in (y_copies, pair_copies, fwd_copies):
-        for copy in copies.values():
-            copy.wait_send()
-    for copy in back_copies.values():
-        copy.wait()
+    block = back.at[pl.ds(0, dp - 1)]
+    remote(block, block, back_sem.at[0], back_sem.at[1], dp=mine).wait_recv()
     square = jnp.zeros((rows, 1), F32)
     for s in range(dp):
         cols = slice(s * w_cols, (s + 1) * w_cols)
@@ -523,6 +507,26 @@
     for s in range(dp):
         cols = slice(s * w_cols, (s + 1) * w_cols)
         normed_ref[:, cols] = (mixed_ref[:, cols] * factor * norm_in[:, cols]).astype(BF16)
+
+    def drain():
+        kv_line.drain(lambda count: kv.at[:, pl.ds(0, count * across * rows), :])
+        w_line.drain(lambda count: w_full.at[pl.ds(0, count * w_rows)])
+        block = w_full.at[pl.ds(0, depth * (across - 1) * w_rows)]
+        whole = [
+            (block, wx_send.at[0]),
+            (stage.at[pl.ds(0, across - 1)], kvx_send.at[0]),
+            (q_stage, qx_send.at[0]),
+            (swap, ax_send.at[0]),
+            (att.at[mine], pair_sem.at[0]),
+            (proj.at[pl.ds(0, dp - 1)], back_sem.at[0]),
+        ]
+        if ny > 1:
+            whole.append((att.at[pl.ds(0, ny - 1)], y_send.at[0]))
+            whole.append((att.at[pl.ds(0, ny - 1)], fwd_sem.at[0]))
+        for block, sem in whole:
+            remote(block, block, sem, back_sem.at[1], sp=me).wait_send()
+
+    return drain
 
 
 class Experts:
@@ -540,7 +544,6 @@
             self.served,
             self.answer,
             self.given,
-            self.acc,
             self.hidden,
             self.partial,
             self.incoming,
@@ -571,7 +574,6 @@
         self.rows, self.model = self.normed.shape
         self.width = self.model // CHUNKS
         self.share = 2 * capacity
-        self.started = []
 
     def role(self, inner):
         return self.inner == inner
@@ -599,16 +601,9 @@
     def cols(self, c):
         return slice(c * self.width, (c + 1) * self.width)
 
-    def send(self, make, inner=None):
-        if inner is None:
-            make().start()
-        else:
-
-            @pl.when(self.role(inner))
-            def _():
-                make().start()
-
-        self.started.append((make, inner))
+    def tables_all(self):
+        block = self.tables.at[pl.ds(0, self.depth - 1)]
+        return self.remote(block, block, self.table_sem.at[0], self.table_sem.at[1], self.at(0))
 
     def prepare(self, phase):
         planes = self.depth
@@ -618,8 +613,8 @@
             return self.remote(
                 self.tables.at[self.z],
                 self.tables.at[self.z],
-                self.table_sem.at[0, d],
-                self.table_sem.at[1, d],
+                self.table_sem.at[0],
+                self.table_sem.at[1],
                 target * self.columns + self.x,
             )
 
@@ -629,10 +624,9 @@
                 [self.routes[...].astype(F32), self.gates[...], jnp.zeros((4, rows), F32)], axis=0
             )
             for d in range(1, planes):
-                self.send(functools.partial(table_copy, d))
+                table_copy(d).start()
             return
-        for d in range(1, planes):
-            table_copy(d).wait_recv()
+        self.tables_all().wait_recv()
         for r in range(planes):
             choice, high, low = selection(
                 self.tables[self.plane(r)],
@@ -657,11 +651,11 @@
         src = self.normed.at[:, cols] if source is None else self.column.at[source - 1, :, cols]
         if place is None:
             place = 1 + 2 * self.inner
-        index = ("forth", "back", 1, 2, 3).index(kind)
+        index = {"forth": 0, "back": 1}.get(kind, 2)
         return self.remote(
             src,
             self.column.at[place - 1, :, cols],
-            self.column_send.at[index, c],
+            self.column_send.at[index],
             self.column_recv.at[place - 1, c],
             self.at(step * self.way),
         )
@@ -671,7 +665,7 @@
         self.remote(
             self.column.at[r - 1, :, cols],
             self.column.at[r - 1, :, cols],
-            self.column_send.at[0, c],
+            self.column_send.at[0],
             self.column_recv.at[r - 1, c],
             self.at(0),
         ).wait_recv()
@@ -681,8 +675,8 @@
         return self.remote(
             self.asked.at[r, pl.ds((k - 1) * self.share, self.share), cols],
             self.served.at[r, pl.ds((self.columns - k) * self.share, self.share), cols],
-            self.ask_send.at[r, c, k],
-            self.ask_recv.at[r, c, self.columns - k],
+            self.ask_send.at[0],
+            self.ask_recv.at[r],
             self.beside(k),
         )
 
@@ -691,57 +685,40 @@
         return self.remote(
             self.given.at[r, pl.ds((k - 1) * self.share, self.share), cols],
             self.answer.at[r, pl.ds((self.columns - k) * self.share, self.share), cols],
-            self.give_send.at[r, c, k],
-            self.give_recv.at[r, c, self.columns - k],
+            self.give_send.at[0],
+            self.give_recv.at[r, c],
             self.beside(k),
         )
 
-    def ask(self, r, c, inner=None):
-        def body():
-            cols = self.cols(c)
-            if r > 0:
-                self.column_arrive(r, c)
-            if r > 0 and inner != 0:
-
-                @pl.when(self.role(1))
-                def _():
-                    self.column_copy(r, c).start()
-
-            lines = self.normed[:, cols] if r == 0 else self.column[r - 1, :, cols]
-            chosen = jnp.dot(self.pick[r], lines, preferred_element_type=F32).astype(BF16)
-            self.served[r, 0 : self.share, cols] = chosen[0 : self.share]
-            for k in range(1, self.columns):
-                part = slice((k - 1) * self.share, k * self.share)
-                self.asked[r, part, cols] = chosen[k * self.share : (k + 1) * self.share]
-                self.ask_copy(r, c, k).start()
-
-        if inner is None:
-            body()
-        else:
-            pl.when(self.role(inner))(body)
-
-    def serve_up(self, r, h):
-        for c in range(h * CHUNKS // 2, (h + 1) * CHUNKS // 2):
-            for k in range(1, self.columns):
-                self.ask_copy(r, c, self.columns - k).wait_recv()
-        if r == 0 and h == 0:
+    def ask(self, inner, r, c):
+        cols = self.cols(c)
+        if r > 0:
+            self.column_arrive(r, c)
+            if inner == 1:
+                self.column_copy(r, c).start()
+        lines = self.normed[:, cols] if r == 0 else self.column[r - 1, :, cols]
+        chosen = jnp.dot(self.pick[r], lines, preferred_element_type=F32).astype(BF16)
+        self.served[r, 0 : self.share, cols] = chosen[0 : self.share]
+        for k in range(1, self.columns):
+            part = slice((k - 1) * self.share, k * self.share)
+            self.asked[r, part, cols] = chosen[k * self.share : (k + 1) * self.share]
+            self.ask_copy(r, c, k).start()
+
+    def serve_up(self, r):
+        block = self.asked.at[r]
+        self.remote(
+            block, block, self.ask_send.at[0], self.ask_recv.at[r], self.at(0)
+        ).wait_recv()
+        if r == 0:
             self.loads[0].wait()
             self.loads[1].wait()
-        deep = slice(h * self.model // 2, (h + 1) * self.model // 2)
-        acc = self.acc
 
         def up_tile(t, carry):
             cols = pl.ds(pl.multiple_of(t * TILE, TILE), TILE)
-            lines = self.served[r, :, deep]
-            gate = jnp.dot(lines, self.gate[deep, cols], preferred_element_type=F32)
-            up = jnp.dot(lines, self.up[deep, cols], preferred_element_type=F32)
-            if h == 0:
-                acc[0, :, cols] = gate
-                acc[1, :, cols] = up
-            else:
-                gate = gate + acc[0, :, cols]
-                up = up + acc[1, :, cols]
-                self.hidden[:, cols] = (gate / (1.0 + jnp.exp(-gate)) * up).astype(BF16)
+            lines = self.served[r]
+            gate = jnp.dot(lines, self.gate[:, cols], preferred_element_type=F32)
+            up = jnp.dot(lines, self.up[:, cols], preferred_element_type=F32)
+            self.hidden[:, cols] = (gate / (1.0 + jnp.exp(-gate)) * up).astype(BF16)
             return carry
 
         lax.fori_loop(0, self.gate.shape[1] // TILE, up_tile, 0)
@@ -764,8 +741,10 @@
             self.give_copy(r, c, k).start()
 
     def combine(self, r, c):
-        for k in range(1, self.columns):
-            self.give_copy(r, c, self.columns - k).wait_recv()
+        block = self.given.at[r, :, self.cols(c)]
+        self.remote(
+            block, block, self.give_send.at[0], self.give_recv.at[r, c], self.at(0)
+        ).wait_recv()
         lines = self.answer[r, :, self.cols(c)]
         return jnp.dot(self.high[r], lines, preferred_element_type=F32) + jnp.dot(
             self.low[r], lines, preferred_element_type=F32
@@ -776,7 +755,7 @@
         return self.remote(
             self.partial.at[slot, :, cols],
             self.incoming.at[place, :, cols],
-            self.part_send.at[slot, c],
+            self.part_send.at[0],
             self.part_recv.at[place, c],
             self.at(step * self.way),
         )
@@ -786,131 +765,129 @@
         self.remote(
             self.partial.at[0, :, cols],
             self.incoming.at[place, :, cols],
-            self.part_send.at[0, c],
+            self.part_send.at[0],
             self.part_recv.at[place, c],
             self.at(0),
         ).wait_recv()
         return self.incoming[place, :, cols].astype(F32)
 
-    def merge(self, inner, r, c, slot, place, step, feed=None):
-        @pl.when(self.role(inner))
-        def _():
-            total = self.combine(r, c)
-            if feed is not None:
-                total = total + self.part_arrive(feed, c)
-            self.partial[slot, :, self.cols(c)] = total.astype(BF16)
-            self.part_copy(slot, place, step, c).start()
+    def merge(self, r, c, slot, place, step, feed=None):
+        total = self.combine(r, c)
+        if feed is not None:
+            total = total + self.part_arrive(feed, c)
+        self.partial[slot, :, self.cols(c)] = total.astype(BF16)
+        self.part_copy(slot, place, step, c).start()
 
     def own(self, c):
         cols = self.cols(c)
         self.hold[:, cols] = self.mixed[:, cols] + self.combine(0, c)
 
-    def finish(self, inner, places):
-        @pl.when(self.role(inner))
-        def _():
-            for c in range(CHUNKS):
-                cols = self.cols(c)
-                total = self.hold[:, cols]
-                for place in places:
-                    total = total + self.part_arrive(place, c)
-                self.result[:, cols] = total.astype(BF16)
-                self.out_copy(c).start()
+    def finish(self, c, places):
+        cols = self.cols(c)
+        total = self.hold[:, cols]
+        for place in places:
+            total = total + self.part_arrive(place, c)
+        self.result[:, cols] = total.astype(BF16)
+        self.out_copy(c).start()
 
     def out_copy(self, c):
         cols = self.cols(c)
         return pltpu.make_async_copy(
-            self.result.at[:, cols], self.out.at[:, cols], self.out_sem.at[c]
-        )
-
-    def run(self):
+            self.result.at[:, cols], self.out.at[:, cols], self.out_sem.at[0]
+        )
+
+    def edge(self):
+        chunks = range(CHUNKS)
+        ask = functools.partial(self.ask, 0)
+
+        def toward(r, c):
+            self.merge(r, c, r - 1, r - 1, 1)
+
+        for c in chunks:
+            self.column_copy("forth", c).start()
+        for c in chunks:
+            ask(0, c)
+        for c in chunks:
+            ask(1, c)
+        self.serve_up(0)
+        for c in chunks:
+            self.serve_down(0, c)
+        self.serve_up(1)
+        for c in chunks:
+            self.serve_down(1, c)
+        ask(2, 0)
+        ask(2, 1)
+        toward(1, 0)
+        ask(2, 2)
+        for c in range(1, CHUNKS):
+            toward(1, c)
+        ask(2, 3)
+        self.serve_up(2)
+        for c in chunks:
+            self.serve_down(2, c)
+        ask(3, 0)
+        ask(3, 1)
+        toward(2, 0)
+        ask(3, 2)
+        for c in range(1, CHUNKS):
+            toward(2, c)
+        ask(3, 3)
+        for c in chunks:
+            self.own(c)
+        self.serve_up(3)
+        for c in chunks:
+            self.serve_down(3, c)
+        for c in chunks:
+            toward(3, c)
+        for c in chunks:
+            self.finish(c, (5,))
+
+    def inside(self):
         chunks = range(CHUNKS)
         half = CHUNKS // 2
-
-        def forth(cs):
-            for c in cs:
-                self.column_copy("forth", c).start()
-
-        for c in chunks:
-
-            @pl.when(self.role(1))
-            def _():
-                self.column_copy("back", c).start()
-
+        ask = functools.partial(self.ask, 1)
+        for c in chunks:
+            self.column_copy("back", c).start()
             if c < half:
                 self.column_copy("forth", c).start()
-            else:
-
-                @pl.when(self.role(0))
-                def _():
-                    self.column_copy("forth", c).start()
-
-        for c in chunks:
-            self.ask(0, c)
-        self.ask(1, 0)
-        self.serve_up(0, 0)
-        self.ask(1, 1)
-        self.serve_up(0, 1)
-        self.ask(1, 2)
-        self.ask(2, 0, 1)
-        self.serve_up(1, 0)
-        self.ask(1, 3)
-
-        @pl.when(self.role(1))
-        def _():
-            forth(range(half, CHUNKS))
-
-        self.ask(2, 1, 1)
-        for c in chunks:
-            self.serve_down(0, c)
-        self.ask(2, 0, 0)
-        self.ask(2, 2, 1)
-        self.serve_up(1, 1)
+        for c in chunks:
+            ask(0, c)
+        ask(1, 0)
+        self.serve_up(0)
+        ask(1, 1)
+        self.serve_down(0, 0)
+        self.serve_down(0, 1)
+        ask(2, 0)
+        ask(1, 2)
+        self.serve_down(0, 2)
+        self.serve_down(0, 3)
+        ask(2, 1)
+        ask(1, 3)
+        for c in range(half, CHUNKS):
+            self.column_copy("forth", c).start()
+        ask(2, 2)
+        ask(2, 3)
+        ask(3, 0)
+        ask(3, 1)
+        self.serve_up(1)
         self.serve_down(1, 0)
         self.serve_down(1, 1)
-        self.ask(2, 1, 0)
-        self.ask(2, 3, 1)
+        ask(3, 2)
         self.serve_down(1, 2)
         self.serve_down(1, 3)
-        self.ask(3, 0, 1)
-        self.ask(3, 1, 1)
-        self.ask(2, 2, 0)
-        self.merge(0, 1, 0, 0, 0, 1)
-        self.merge(0, 1, 1, 0, 0, 1)
-        self.serve_up(2, 0)
-        self.ask(2, 3, 0)
-        self.ask(3, 2, 1)
-        self.merge(0, 1, 2, 0, 0, 1)
-        self.merge(0, 1, 3, 0, 0, 1)
-        self.ask(3, 0, 0)
-        self.ask(3, 3, 1)
-        self.serve_up(2, 1)
-        self.serve_down(2, 0)
-        self.serve_down(2, 1)
-        self.ask(3, 1, 0)
-        self.serve_down(2, 2)
-        self.serve_down(2, 3)
-        self.ask(3, 2, 0)
-        self.merge(0, 2, 0, 1, 1, 1)
-        self.merge(0, 2, 1, 1, 1, 1)
-        self.serve_up(3, 0)
-        self.ask(3, 3, 0)
-        self.merge(0, 2, 2, 1, 1, 1)
-        self.merge(0, 2, 3, 1, 1, 1)
-        self.own(0)
-        self.own(1)
-        self.serve_up(3, 1)
-        for c in chunks:
-            self.serve_down(3, c)
-        for c in chunks:
-            self.merge(0, 3, c, 2, 2, 1)
-        self.own(2)
-        self.own(3)
+        ask(3, 3)
+        for r in (2, 3):
+            self.serve_up(r)
+            for c in chunks:
+                self.serve_down(r, c)
+        for c in chunks:
+            self.own(c)
 
         def far(c):
-            self.merge(1, 2, c, 1, 3, 1, 1)
+            self.merge(2, c, 1, 3, 1, 1)
 
         def near(c):
-            self.merge(1, 1, c, 3, 5, -1, 3)
+            self.merge(1, c, 3, 5, -1, 3)
 
         for c in chunks:
             far(c)
@@ -918,42 +895,38 @@
                 near(c - 1)
         near(CHUNKS - 1)
         for c in chunks:
-            self.merge(1, 3, c, 2, 4, 1, 2)
-        self.finish(0, (5,))
-        self.finish(1, (0, 4))
-        self.drain()
-
-    def drain(self):
-        for make, _ in self.started:
-            make().wait_send()
-        for c in range(CHUNKS):
-            self.column_copy("forth", c).wait_send()
-
-            @pl.when(self.role(1))
-            def _():
-                self.column_copy("back", c).wait_send()
-                for r in (1, 2, 3):
-                    self.column_copy(r, c).wait_send()
-                for slot, place, step in ((1, 3, 1), (2, 4, 1), (3, 5, -1)):
-                    self.part_copy(slot, place, step, c).wait_send()
-
-            @pl.when(self.role(0))
-            def _():
-                for slot in range(3):
-                    self.part_copy(slot, slot, 1, c).wait_send()
-
-            for r in range(self.depth):
-                for k in range(1, self.columns):
-                    self.ask_copy(r, c, k).wait_send()
-                    self.give_copy(r, c, k).wait_send()
-            self.out_copy(c).wait()
+            self.merge(3, c, 2, 4, 1, 2)
+        for c in chunks:
+            self.finish(c, (0, 4))
+
+    def run(self):
+        pl.when(self.role(0))(self.edge)
+        pl.when(self.role(1))(self.inside)
+        ends = [
+            (self.normed, self.column_send.at[0]),
+            (self.asked, self.ask_send.at[0]),
+            (self.given, self.give_send.at[0]),
+            (self.partial.at[pl.ds(0, 3)], self.part_send.at[0]),
+        ]
+        for block, sem in ends:
+            self.remote(block, block, sem, self.part_recv.at[0, 0], self.at(0)).wait_send()
+
+        @pl.when(self.role(1))
+        def _():
+            for block, way in ((self.normed, 1), (self.column, 2)):
+                self.remote(
+                    block, block, self.column_send.at[way], self.part_recv.at[0, 0], self.at(0)
+                ).wait_send()
+
+        self.tables_all().wait_send()
+        pltpu.make_async_copy(self.result, self.out, self.out_sem.at[0]).wait()
 
 
 def layer_kernel(n, dp, capacity, *refs):
     inputs, refs = refs[:10], refs[10:]
     weights, out_ref, refs = refs[:3], refs[3], refs[4:]
     middle, refs = refs[:2], refs[2:]
-    attention, refs = refs[:37], refs[37:]
+    attention, refs = refs[:34], refs[34:]
     load_sem, stores = refs[0], refs[1:4]
     loads = [
         pltpu.make_async_copy(src.at[0], dst, load_sem.at[i])
@@ -965,8 +938,9 @@
             load.start()
 
     experts = Experts(n, capacity, *inputs[8:], middle, loads, out_ref, *refs[1:])
-    attention_part(n, dp, start_loads, *inputs[:8], *middle, experts.prepare, *attention)
+    drain = attention_part(n, dp, start_loads, *inputs[:8], *middle, experts.prepare, *attention)
     experts.run()
+    drain()
 
 
 def on_device(
@@ -1020,26 +994,23 @@
         pltpu.VMEM((2, 1, width), F32),
         pltpu.VMEM((1, model), F32),
         dma((8,)),
-        dma((across, local_kv)),
-        dma((across, local_kv)),
-        dma((units, depth, 2)),
+        dma((1,)),
+        dma((across - 1, local_kv)),
+        dma((2,)),
         dma((units, depth)),
-        dma((across,)),
-        dma((across,)),
-        dma((4, depth, across)),
-        dma((4, depth, across)),
-        dma((4, depth, 2)),
+        dma((1,)),
+        dma((1,)),
+        dma((1,)),
+        dma((2,)),
+        dma((2,)),
         dma((4, depth)),
-        dma((across, local_kv)),
-        dma((across, local_kv)),
-        dma((ny, units)),
-        dma((ny, units)),
-        dma((units,)),
-        dma((units,)),
-        dma((ny, units)),
-        dma((ny, units)),
-        dma((dp, 2)),
-        dma((dp, 2)),
+        dma((1,)),
+        dma((across - 1, local_kv)),
+        dma((1,)),
+        dma((max(1, ny - 1), units)),
+        dma((2,)),
+        dma((2,)),
+        dma((2,)),
     ]
     result = pl.pallas_call(
         functools.partial(layer_kernel, n, dp, capacity),
@@ -1063,22 +1034,21 @@
             pltpu.VMEM((depth, slots, model), BF16),
             pltpu.VMEM((depth, slots, model), BF16),
             pltpu.VMEM((depth, aside, model), BF16),
-            pltpu.VMEM((2, slots, ff), F32),
             pltpu.VMEM((slots, ff), BF16),
             pltpu.VMEM((4, rows, model), BF16),
             pltpu.VMEM((6, rows, model), BF16),
             pltpu.VMEM((rows, model), F32),
             pltpu.VMEM((rows, model), BF16),
-            dma((2, depth)),
-            dma((5, CHUNKS)),
+            dma((2,)),
+            dma((3,)),
             dma((depth - 1, CHUNKS)),
-            dma((depth, CHUNKS, across)),
-            dma((depth, CHUNKS, across)),
-            dma((depth, CHUNKS, across)),
-            dma((depth, CHUNKS, across)),
-            dma((4, CHUNKS)),
+            dma((1,)),
+            dma((depth,)),
+            dma((1,)),
+            dma((depth, CHUNKS)),
+            dma((1,)),
             dma((6, CHUNKS)),
-            dma((CHUNKS,)),
+            dma((1,)),
         ],
         compiler_params=pltpu.CompilerParams(
             collective_id=0, has_side_effects=True, vmem_limit_bytes=56 * 1024 * 1024

time: 133 us -> 131 us (0.985)
  no operation moved by 1% of the time
where the time goes in v3:
time: 131 us
  Pallas kernels  129 us (98%)
  local copies, waits for them, and re-layouts  1.88 us (1%)
    pallas_call x1, Pallas kernels, on_device(): pl.pallas_call(functools.partial(layer_kernel, n, dp, capacity), out_shap...  129 us

profile of v3, /device:TPU:8, one launch (start us, length us, event | category | flops | bytes accessed | tf_op | source)
XLA Modules:
  0.0 130.6 jit_solution(13572877127910700675)
XLA Ops:
  0.0 128.7 %layer.1 = bf16[128,2048]{1,0:T(8,128)(2,1)} custom-call(bf16[128,16,128]{2,1,0:T(8,128)(2,1)} %bitcast.15, bf16[128,4,128]{2,1,0:T(4,128)(2,1)} %bitcast.17, bf16[128,4,128]{2,1,0:T(4,128)(2,1)} %bitcast.18, f32[1,128]{1,0:T(1,128)} %bitcast.22, f32[1,128]{1,0:T(1,128)} %bitcast.23, bf16[256,512]{1,0:T(8,128)(2,1)} %refs_5_.1, bf16[128,2048]{1,0:T(8,128)(2,1)} %bitcast.16, ...), custom_call_target="tpu_custom_call" | custom-call | tf_op jit(solution)/shard_map/layer/pallas_call | solution.py:1015
  128.7 1.9 %copy.15 = bf16[1,128,2048]{2,1,0:T(8,128)(2,1)} copy(bf16[1,128,2048]{2,1,0:T(8,128)(2,1)} %bitcast.14) | data formatting | bytes 1048576

commit v4 on v3

--- a/solution.py
+++ b/solution.py
@@ -172,6 +172,7 @@
     qx_recv,
     wx_send,
     wx_recv,
+    wo_sem,
     wz_send,
     wz_recv,
     ax_send,
@@ -343,10 +344,41 @@
                 remote(
                     w_unit(u, plane * across + x),
                     w_unit(u, plane * across + x),
-                    wx_send.at[0],
-                    wx_recv.at[w_units[u][0]],
+                    wx_send.at[w_units[u][0]],
+                    wx_recv.at[w_units[u][0]] if plane is not z else wo_sem.at[0],
                     sp=beside(k),
                 ).start()
+
+    upper = z // (depth // 2)
+    way = 1 - 2 * upper
+    middle = (z > 0) & (z < depth - 1)
+    edge = jnp.logical_not(middle)
+
+    def w_half(sp, j):
+        return w_full.at[span(sp, w_rows), pl.ds(j * part_cols, part_cols)]
+
+    def w_along():
+        block = w_full.at[pl.ds(0, (across - 1) * w_rows)]
+        remote(block, block, wo_sem.at[1], wo_sem.at[0], sp=me).wait_recv()
+        for j in range(halves):
+            for k in range(1, across):
+                block = w_half(beside(k), j)
+                target = me + way * across
+                remote(block, block, wo_sem.at[1], wx_recv.at[j], sp=target).start()
+
+        @pl.when(middle)
+        def _():
+            for k in range(1, across):
+                block = w_half(beside(k), 0)
+                target = me - way * across
+                remote(block, block, wo_sem.at[2], wx_recv.at[0], sp=target).start()
+
+    def w_aside(units):
+        def then(condition, u, plane):
+            if w_units[u][0] in units:
+                w_across(condition, u, plane)
+
+        return then
 
     def w_begin(t):
         for u in range(len(w_units)):
@@ -361,7 +393,6 @@
         for u in range(len(kv_units)):
             kv_line.step(t, u)
         w_begin(t)
-    middle = (z > 0) & (z < depth - 1)
     prepare(1)
     remote(
         q_stage,
@@ -406,7 +437,8 @@
                 kv_line.step(depth - 1, u)
         if g == local_kv - 1:
             for u in range(len(w_units)):
-                w_line.step(1, u, middle, w_across)
+                w_line.step(1, u, middle)
+            w_along()
 
         def one_head(i, carry):
             h = g * group + i
@@ -441,7 +473,7 @@
         for u in range(len(w_units)):
             w_line.step(t, u, middle, w_across)
     for u in range(len(w_units)):
-        w_line.step(1, u, jnp.logical_not(middle), w_across)
+        w_line.step(1, u, edge, w_aside((1,)))
     for u, (k, g) in enumerate(kv_units):
         if k == 0:
             continue
@@ -455,7 +487,7 @@
         spread_att(u)
     for t in range(2, depth - 1):
         for u in range(len(w_units)):
-            w_line.step(t, u, jnp.logical_not(middle), w_across)
+            w_line.step(t, u, edge, w_across)
     order = own_units + [u for u in range(len(kv_units)) if u not in own_units]
     for i in range(max(len(order), len(w_units))):
         if i < len(w_units):
@@ -474,7 +506,7 @@
 
     for j in range(halves):
         cols = slice(j * part_cols, (j + 1) * part_cols)
-        block = w_full.at[pl.ds(0, depth * (across - 1) * w_rows), cols]
+        block = w_full.at[pl.ds(0, (depth - 1) * (across - 1) * w_rows), cols]
         remote(block, block, wx_send.at[0], wx_recv.at[j], sp=me).wait_recv()
         result = jnp.dot(
             att[...].reshape(dp * rows, model), w_full[:, cols], preferred_element_type=F32
@@ -511,9 +543,23 @@
     def drain():
         kv_line.drain(lambda count: kv.at[:, pl.ds(0, count * across * rows), :])
         w_line.drain(lambda count: w_full.at[pl.ds(0, count * w_rows)])
-        block = w_full.at[pl.ds(0, depth * (across - 1) * w_rows)]
+        for role, counts in ((edge, (depth - 1, depth)), (middle, (2, 2))):
+
+            @pl.when(role)
+            def _():
+                for j, count in enumerate(counts):
+                    block = w_full.at[
+                        pl.ds(0, count * (across - 1) * w_rows), pl.ds(0, part_cols)
+                    ]
+                    remote(block, block, wx_send.at[j], back_sem.at[1], sp=me).wait_send()
+
+        @pl.when(middle)
+        def _():
+            block = w_full.at[pl.ds(0, (across - 1) * w_rows), pl.ds(0, part_cols)]
+            remote(block, block, wo_sem.at[2], back_sem.at[1], sp=me).wait_send()
+
         whole = [
-            (block, wx_send.at[0]),
+            (w_full.at[pl.ds(0, (across - 1) * w_rows)], wo_sem.at[1]),
             (stage.at[pl.ds(0, across - 1)], kvx_send.at[0]),
             (q_stage, qx_send.at[0]),
             (swap, ax_send.at[0]),
@@ -704,12 +750,12 @@
             self.asked[r, part, cols] = chosen[k * self.share : (k + 1) * self.share]
             self.ask_copy(r, c, k).start()
 
-    def serve_up(self, r):
+    def serve_up(self, r, first=False):
         block = self.asked.at[r]
         self.remote(
             block, block, self.ask_send.at[0], self.ask_recv.at[r], self.at(0)
         ).wait_recv()
-        if r == 0:
+        if first:
             self.loads[0].wait()
             self.loads[1].wait()
 
@@ -718,19 +764,19 @@
             lines = self.served[r]
             gate = jnp.dot(lines, self.gate[:, cols], preferred_element_type=F32)
             up = jnp.dot(lines, self.up[:, cols], preferred_element_type=F32)
-            self.hidden[:, cols] = (gate / (1.0 + jnp.exp(-gate)) * up).astype(BF16)
+            self.hidden[min(r, 1), :, cols] = (gate / (1.0 + jnp.exp(-gate)) * up).astype(BF16)
             return carry
 
         lax.fori_loop(0, self.gate.shape[1] // TILE, up_tile, 0)
 
-    def serve_down(self, r, c):
-        if r == 0 and c == 0:
+    def serve_down(self, r, c, first=False):
+        if first:
             self.loads[2].wait()
 
         def down_tile(t, carry):
             cols = pl.ds(pl.multiple_of(c * self.width + t * TILE, TILE), TILE)
             lines = jnp.dot(
-                self.hidden[...], self.down[:, cols], preferred_element_type=F32
+                self.hidden[min(r, 1)], self.down[:, cols], preferred_element_type=F32
             ).astype(BF16)
             self.answer[r, 0 : self.share, cols] = lines[0 : self.share]
             self.given[r, :, cols] = lines[self.share :]
@@ -803,83 +849,78 @@
         def toward(r, c):
             self.merge(r, c, r - 1, r - 1, 1)
 
+        def down(r, *cs):
+            for c in cs:
+                self.serve_down(r, c, r == 1 and c == 0)
+
         for c in chunks:
             self.column_copy("forth", c).start()
         for c in chunks:
+            ask(1, c)
+        for c in chunks:
             ask(0, c)
-        for c in chunks:
-            ask(1, c)
-        self.serve_up(0)
-        for c in chunks:
-            self.serve_down(0, c)
-        self.serve_up(1)
-        for c in chunks:
-            self.serve_down(1, c)
+        self.serve_up(1, True)
+        down(1, *chunks)
         ask(2, 0)
+        toward(1, 0)
         ask(2, 1)
-        toward(1, 0)
+        toward(1, 1)
+        toward(1, 2)
         ask(2, 2)
-        for c in range(1, CHUNKS):
-            toward(1, c)
+        toward(1, 3)
         ask(2, 3)
-        self.serve_up(2)
-        for c in chunks:
-            self.serve_down(2, c)
         ask(3, 0)
         ask(3, 1)
+        self.serve_up(0)
+        ask(3, 2)
+        ask(3, 3)
+        self.serve_up(2)
+        down(2, *chunks)
         toward(2, 0)
-        ask(3, 2)
-        for c in range(1, CHUNKS):
-            toward(2, c)
-        ask(3, 3)
-        for c in chunks:
-            self.own(c)
+        toward(2, 1)
         self.serve_up(3)
-        for c in chunks:
-            self.serve_down(3, c)
+        toward(2, 2)
+        toward(2, 3)
+        down(3, *chunks)
+        down(0, *chunks)
         for c in chunks:
             toward(3, c)
         for c in chunks:
+            self.own(c)
+        for c in chunks:
             self.finish(c, (5,))
 
     def inside(self):
         chunks = range(CHUNKS)
-        half = CHUNKS // 2
         ask = functools.partial(self.ask, 1)
+
+        def down(r, *cs):
+            for c in cs:
+                self.serve_down(r, c, r == 0 and c == 0)
+
         for c in chunks:
             self.column_copy("back", c).start()
-            if c < half:
-                self.column_copy("forth", c).start()
+            self.column_copy("forth", c).start()
         for c in chunks:
             ask(0, c)
+        ask(3, 0)
+        self.serve_up(0, True)
         ask(1, 0)
-        self.serve_up(0)
+        down(0, 0, 1)
         ask(1, 1)
-        self.serve_down(0, 0)
-        self.serve_down(0, 1)
         ask(2, 0)
+        down(0, 2, 3)
         ask(1, 2)
-        self.serve_down(0, 2)
-        self.serve_down(0, 3)
         ask(2, 1)
         ask(1, 3)
-        for c in range(half, CHUNKS):
-            self.column_copy("forth", c).start()
         ask(2, 2)
         ask(2, 3)
-        ask(3, 0)
         ask(3, 1)
-        self.serve_up(1)
-        self.serve_down(1, 0)
-        self.serve_down(1, 1)
         ask(3, 2)
-        self.serve_down(1, 2)
-        self.serve_down(1, 3)
         ask(3, 3)
-        for r in (2, 3):
+        for r in (1, 2, 3):
             self.serve_up(r)
-            for c in chunks:
-                self.serve_down(r, c)
+            down(r, *chunks)
         for c in chunks:
             self.own(c)
 
@@ -926,7 +967,7 @@
     inputs, refs = refs[:10], refs[10:]
     weights, out_ref, refs = refs[:3], refs[3], refs[4:]
     middle, refs = refs[:2], refs[2:]
-    attention, refs = refs[:34], refs[34:]
+    attention, refs = refs[:35], refs[35:]
     load_sem, stores = refs[0], refs[1:4]
     loads = [
         pltpu.make_async_copy(src.at[0], dst, load_sem.at[i])
@@ -1000,8 +1041,9 @@
         dma((units, depth)),
         dma((1,)),
         dma((1,)),
-        dma((1,)),
         dma((2,)),
+        dma((2,)),
+        dma((3,)),
         dma((2,)),
         dma((4, depth)),
         dma((1,)),
@@ -1034,7 +1076,7 @@
             pltpu.VMEM((depth, slots, model), BF16),
             pltpu.VMEM((depth, slots, model), BF16),
             pltpu.VMEM((depth, aside, model), BF16),
-            pltpu.VMEM((slots, ff), BF16),
+            pltpu.VMEM((2, slots, ff), BF16),
             pltpu.VMEM((4, rows, model), BF16),
             pltpu.VMEM((6, rows, model), BF16),
             pltpu.VMEM((rows, model), F32),

time: 131 us -> 126 us (0.962)
  Pallas kernels: 129 us -> 124 us
    pallas_call x1, Pallas kernels: 129 us -> 124 us  [on_device(): pl.pallas_call(functools.partial(layer_kernel, n, dp, capacity), out_shap...]
where the time goes in v4:
time: 126 us; the launch traced here: 125 us
  Pallas kernels  124 us (98%)
  local copies, waits for them, and re-layouts  1.88 us (1%)
    pallas_call x1, Pallas kernels, on_device(): pl.pallas_call(functools.partial(layer_kernel, n, dp, capacity), out_shap...  124 us

profile of v4, /device:TPU:8, one launch (start us, length us, event | category | flops | bytes accessed | tf_op | source)
XLA Modules:
  0.0 125.4 jit_solution(4038588540318431230)
XLA Ops:
  0.0 123.5 %layer.1 = bf16[128,2048]{1,0:T(8,128)(2,1)} custom-call(bf16[128,16,128]{2,1,0:T(8,128)(2,1)} %bitcast.15, bf16[128,4,128]{2,1,0:T(4,128)(2,1)} %bitcast.17, bf16[128,4,128]{2,1,0:T(4,128)(2,1)} %bitcast.18, f32[1,128]{1,0:T(1,128)} %bitcast.22, f32[1,128]{1,0:T(1,128)} %bitcast.23, bf16[256,512]{1,0:T(8,128)(2,1)} %refs_5_.1, bf16[128,2048]{1,0:T(8,128)(2,1)} %bitcast.16, ...), custom_call_target="tpu_custom_call" | custom-call | tf_op jit(solution)/shard_map/layer/pallas_call | solution.py:1057
  123.5 1.9 %copy.15 = bf16[1,128,2048]{2,1,0:T(8,128)(2,1)} copy(bf16[1,128,2048]{2,1,0:T(8,128)(2,1)} %bitcast.14) | data formatting | bytes 1048576

commit v5 on v4

--- a/solution.py
+++ b/solution.py
@@ -146,7 +146,7 @@
     ng_ref,
     mixed_ref,
     normed_ref,
-    prepare,
+    experts,
     q_in,
     k_in,
     v_in,
@@ -181,7 +181,8 @@
     y_recv,
     pair_sem,
     fwd_sem,
-    back_sem,
+    back_send,
+    back_recv,
 ):
     me = lax.axis_index("sp")
     mine = lax.axis_index("dp")
@@ -351,6 +352,11 @@
 
     upper = z // (depth // 2)
     way = 1 - 2 * upper
+
+    def block_of(i, step):
+        row = lax.rem(row_y + ny + step * (i // 2), ny)
+        return row * 2 + (core if i % 2 == 0 else 1 - core)
+
     middle = (z > 0) & (z < depth - 1)
     edge = jnp.logical_not(middle)
 
@@ -386,14 +392,14 @@
             w_line.down(depth - 1 - z == t, u, z)
 
     w_begin(0)
-    prepare(0)
+    experts.prepare(0)
     for u in range(len(w_units)):
         w_across(always, u, z)
     for t in range(1, depth - 1):
         for u in range(len(kv_units)):
             kv_line.step(t, u)
         w_begin(t)
-    prepare(1)
+    experts.prepare(1)
     remote(
         q_stage,
         q_all.at[:, pl.ds(rows, (across - 1) * rows), :],
@@ -514,31 +520,41 @@
         for s in range(dp):
             proj[s, :, cols] = result[s * rows : (s + 1) * rows]
         back[mine, :, cols] = proj[mine, :, cols]
-        order = sorted(range(1, dp), key=lambda d: d % 2)
-        for d in order:
-            target = lax.rem(mine + d, dp)
+        for i in list(range(2, dp)) + [1]:
+            target = block_of(i, 1)
             remote(
                 proj.at[target, :, cols],
                 back.at[mine, :, cols],
-                back_sem.at[0],
-                back_sem.at[1],
+                back_send.at[0],
+                back_recv.at[i],
                 dp=target,
             ).start()
 
     fetches[6].wait()
     fetches[7].wait()
-    block = back.at[pl.ds(0, dp - 1)]
-    remote(block, block, back_sem.at[0], back_sem.at[1], dp=mine).wait_recv()
     square = jnp.zeros((rows, 1), F32)
-    for s in range(dp):
-        cols = slice(s * w_cols, (s + 1) * w_cols)
-        part = res_in[:, cols].astype(F32) + back[s].astype(F32)
+    each = dp // CHUNKS
+    for i in range(dp):
+        source = block_of(i, -1)
+        if i > 0:
+            remote(back.at[mine], back.at[source], back_send.at[0], back_recv.at[i], dp=mine).wait_recv()
+        cols = span(source, w_cols)
+        part = res_in[:, cols].astype(F32) + back[source].astype(F32)
         mixed_ref[:, cols] = part
         square = square + jnp.sum(part * part, axis=-1, keepdims=True)
-    factor = lax.rsqrt(square / model + EPS)
-    for s in range(dp):
-        cols = slice(s * w_cols, (s + 1) * w_cols)
-        normed_ref[:, cols] = (mixed_ref[:, cols] * factor * norm_in[:, cols]).astype(BF16)
+        normed_ref[:, i * w_cols : (i + 1) * w_cols] = part.astype(BF16)
+        if i == dp - 1:
+            factor = lax.rsqrt(square / model + EPS)
+            high = factor.astype(BF16).astype(F32)
+            mid = (factor - high).astype(BF16).astype(F32)
+            lane = lax.broadcasted_iota(jnp.int32, (rows, width), 1)
+            pieces = jnp.where(lane == 0, high, jnp.where(lane == 1, mid, 0.0))
+            pieces = jnp.where(lane == 2, factor - high - mid, pieces)
+            normed_ref[:, model : model + width] = pieces.astype(BF16)
+        if i % each == each - 1:
+            experts.launch(i // each)
+        if i == dp // 2 - 1:
+            experts.early()
 
     def drain():
         kv_line.drain(lambda count: kv.at[:, pl.ds(0, count * across * rows), :])
@@ -551,12 +567,12 @@
                     block = w_full.at[
                         pl.ds(0, count * (across - 1) * w_rows), pl.ds(0, part_cols)
                     ]
-                    remote(block, block, wx_send.at[j], back_sem.at[1], sp=me).wait_send()
+                    remote(block, block, wx_send.at[j], back_recv.at[0], sp=me).wait_send()
 
         @pl.when(middle)
         def _():
             block = w_full.at[pl.ds(0, (across - 1) * w_rows), pl.ds(0, part_cols)]
-            remote(block, block, wo_sem.at[2], back_sem.at[1], sp=me).wait_send()
+            remote(block, block, wo_sem.at[2], back_recv.at[0], sp=me).wait_send()
 
         whole = [
             (w_full.at[pl.ds(0, (across - 1) * w_rows)], wo_sem.at[1]),
@@ -564,19 +580,19 @@
             (q_stage, qx_send.at[0]),
             (swap, ax_send.at[0]),
             (att.at[mine], pair_sem.at[0]),
-            (proj.at[pl.ds(0, dp - 1)], back_sem.at[0]),
+            (proj.at[pl.ds(0, dp - 1)], back_send.at[0]),
         ]
         if ny > 1:
             whole.append((att.at[pl.ds(0, ny - 1)], y_send.at[0]))
             whole.append((att.at[pl.ds(0, ny - 1)], fwd_sem.at[0]))
         for block, sem in whole:
-            remote(block, block, sem, back_sem.at[1], sp=me).wait_send()
+            remote(block, block, sem, back_recv.at[0], sp=me).wait_send()
 
     return drain
 
 
 class Experts:
-    def __init__(self, n, capacity, routes, gates, middle, loads, out, *refs):
+    def __init__(self, n, dp, capacity, norm, routes, gates, middle, loads, out, *refs):
         (
             self.gate,
             self.up,
@@ -590,11 +606,11 @@
             self.served,
             self.answer,
             self.given,
+            self.ready,
             self.hidden,
             self.partial,
             self.incoming,
             self.hold,
-            self.result,
             self.table_sem,
             self.column_send,
             self.column_recv,
@@ -604,7 +620,6 @@
             self.give_recv,
             self.part_send,
             self.part_recv,
-            self.out_sem,
         ) = refs
         self.mixed, self.normed = middle
         self.routes, self.gates = routes, gates
@@ -617,7 +632,8 @@
         self.way = 1 - 2 * self.upper
         self.inner = self.upper * (self.depth - 1) + self.way * self.z
         self.capacity = capacity
-        self.rows, self.model = self.normed.shape
+        self.norm, self.dp = norm, dp
+        self.rows, self.model = self.mixed.shape
         self.width = self.model // CHUNKS
         self.share = 2 * capacity
 
@@ -643,6 +659,23 @@
 
     def beside(self, k):
         return self.z * self.columns + (self.x + k) % self.columns
+
+    def lanes(self, c):
+        end = (c + 1) * self.width if c < CHUNKS - 1 else self.normed.shape[1]
+        return slice(c * self.width, end)
+
+    def early(self):
+        @pl.when(self.role(0))
+        def _():
+            for c in range(CHUNKS // 2):
+                self.ask(0, 1, c)
+
+    def launch(self, c):
+        self.column_copy("forth", c).start()
+
+        @pl.when(self.role(1))
+        def _():
+            self.column_copy("back", c).start()
 
     def cols(self, c):
         return slice(c * self.width, (c + 1) * self.width)
@@ -693,7 +726,7 @@
             2: (2, 2, -1),
             3: (3, 3, -1),
         }[kind]
-        cols = self.cols(c)
+        cols = self.lanes(c)
         src = self.normed.at[:, cols] if source is None else self.column.at[source - 1, :, cols]
         if place is None:
             place = 1 + 2 * self.inner
@@ -707,7 +740,7 @@
         )
 
     def column_arrive(self, r, c):
-        cols = self.cols(c)
+        cols = self.lanes(c)
         self.remote(
             self.column.at[r - 1, :, cols],
             self.column.at[r - 1, :, cols],
@@ -717,7 +750,7 @@
         ).wait_recv()
 
     def ask_copy(self, r, c, k):
-        cols = self.cols(c)
+        cols = self.lanes(c)
         return self.remote(
             self.asked.at[r, pl.ds((k - 1) * self.share, self.share), cols],
             self.served.at[r, pl.ds((self.columns - k) * self.share, self.share), cols],
@@ -737,7 +770,7 @@
         )
 
     def ask(self, inner, r, c):
-        cols = self.cols(c)
+        cols = self.lanes(c)
         if r > 0:
             self.column_arrive(r, c)
             if inner == 1:
@@ -759,9 +792,20 @@
             self.loads[0].wait()
             self.loads[1].wait()
 
+        pieces = self.served[r, :, self.model :].astype(F32)
+        factor = jnp.sum(pieces, axis=-1, keepdims=True)
+        mine = lax.axis_index("dp")
+        size = self.model // self.dp
+        for i in range(self.dp):
+            row = (mine // 2 + self.dp // 2 - i // 2) % (self.dp // 2)
+            block = row * 2 + (mine % 2 if i % 2 == 0 else 1 - mine % 2)
+            cols = pl.ds(pl.multiple_of(block * size, size), size)
+            lines = self.served[r, :, i * size : (i + 1) * size].astype(F32)
+            self.ready[:, cols] = (lines * factor * self.norm[:, cols]).astype(BF16)
+
         def up_tile(t, carry):
             cols = pl.ds(pl.multiple_of(t * TILE, TILE), TILE)
-            lines = self.served[r]
+            lines = self.ready[...]
             gate = jnp.dot(lines, self.gate[:, cols], preferred_element_type=F32)
             up = jnp.dot(lines, self.up[:, cols], preferred_element_type=F32)
             self.hidden[min(r, 1), :, cols] = (gate / (1.0 + jnp.exp(-gate)) * up).astype(BF16)
@@ -833,14 +877,7 @@
         total = self.hold[:, cols]
         for place in places:
             total = total + self.part_arrive(place, c)
-        self.result[:, cols] = total.astype(BF16)
-        self.out_copy(c).start()
-
-    def out_copy(self, c):
-        cols = self.cols(c)
-        return pltpu.make_async_copy(
-            self.result.at[:, cols], self.out.at[:, cols], self.out_sem.at[0]
-        )
+        self.out[:, cols] = total.astype(BF16)
 
     def edge(self):
         chunks = range(CHUNKS)
@@ -853,9 +890,7 @@
             for c in cs:
                 self.serve_down(r, c, r == 1 and c == 0)
 
-        for c in chunks:
-            self.column_copy("forth", c).start()
-        for c in chunks:
+        for c in range(CHUNKS // 2, CHUNKS):
             ask(1, c)
         for c in chunks:
             ask(0, c)
@@ -870,17 +905,15 @@
         toward(1, 3)
         ask(2, 3)
         ask(3, 0)
+        self.serve_up(0)
         ask(3, 1)
-        self.serve_up(0)
+        self.serve_up(2)
+        down(2, *chunks)
         ask(3, 2)
         ask(3, 3)
-        self.serve_up(2)
-        down(2, *chunks)
-        toward(2, 0)
-        toward(2, 1)
+        for c in chunks:
+            toward(2, c)
         self.serve_up(3)
-        toward(2, 2)
-        toward(2, 3)
         down(3, *chunks)
         down(0, *chunks)
         for c in chunks:
@@ -899,17 +932,11 @@
                 self.serve_down(r, c, r == 0 and c == 0)
 
         for c in chunks:
-            self.column_copy("back", c).start()
-            self.column_copy("forth", c).start()
-        for c in chunks:
             ask(0, c)
         ask(3, 0)
-        self.serve_up(0, True)
         ask(1, 0)
-        down(0, 0, 1)
         ask(1, 1)
         ask(2, 0)
-        down(0, 2, 3)
         ask(1, 2)
         ask(2, 1)
         ask(1, 3)
@@ -918,8 +945,8 @@
         ask(3, 1)
         ask(3, 2)
         ask(3, 3)
-        for r in (1, 2, 3):
-            self.serve_up(r)
+        for r in (0, 1, 2, 3):
+            self.serve_up(r, r == 0)
             down(r, *chunks)
         for c in chunks:
             self.own(c)
@@ -960,14 +987,13 @@
                 ).wait_send()
 
         self.tables_all().wait_send()
-        pltpu.make_async_copy(self.result, self.out, self.out_sem.at[0]).wait()
 
 
 def layer_kernel(n, dp, capacity, *refs):
     inputs, refs = refs[:10], refs[10:]
     weights, out_ref, refs = refs[:3], refs[3], refs[4:]
     middle, refs = refs[:2], refs[2:]
-    attention, refs = refs[:35], refs[35:]
+    attention, refs = refs[:36], refs[36:]
     load_sem, stores = refs[0], refs[1:4]
     loads = [
         pltpu.make_async_copy(src.at[0], dst, load_sem.at[i])
@@ -978,8 +1004,9 @@
         for load in loads:
             load.start()
 
-    experts = Experts(n, capacity, *inputs[8:], middle, loads, out_ref, *refs[1:])
-    drain = attention_part(n, dp, start_loads, *inputs[:8], *middle, experts.prepare, *attention)
+    norm = attention[15]
+    experts = Experts(n, dp, capacity, norm, *inputs[8:], middle, loads, out_ref, *refs[1:])
+    drain = attention_part(n, dp, start_loads, *inputs[:8], *middle, experts, *attention)
     experts.run()
     drain()
 
@@ -1052,16 +1079,17 @@
         dma((max(1, ny - 1), units)),
         dma((2,)),
         dma((2,)),
-        dma((2,)),
+        dma((1,)),
+        dma((dp,)),
     ]
     result = pl.pallas_call(
         functools.partial(layer_kernel, n, dp, capacity),
-        out_shape=jax.ShapeDtypeStruct((rows, model), BF16),
+        out_shape=pltpu.VMEM((rows, model), BF16),
         in_specs=[ANY] * 8 + [VMEM] * 2 + [ANY] * 3,
-        out_specs=ANY,
+        out_specs=VMEM,
         scratch_shapes=[
             pltpu.VMEM((rows, model), F32),
-            pltpu.VMEM((rows, model), BF16),
+            pltpu.VMEM((rows, model + width), BF16),
             *attention_scratch,
             dma((3,)),
             pltpu.VMEM((model, ff), BF16),
@@ -1071,16 +1099,16 @@
             pltpu.VMEM((depth, slots, rows), BF16),
             pltpu.VMEM((depth, rows, slots), BF16),
             pltpu.VMEM((depth, rows, slots), BF16),
-            pltpu.VMEM((depth - 1, rows, model), BF16),
-            pltpu.VMEM((depth, aside, model), BF16),
-            pltpu.VMEM((depth, slots, model), BF16),
+            pltpu.VMEM((depth - 1, rows, model + width), BF16),
+            pltpu.VMEM((depth, aside, model + width), BF16),
+            pltpu.VMEM((depth, slots, model + width), BF16),
             pltpu.VMEM((depth, slots, model), BF16),
             pltpu.VMEM((depth, aside, model), BF16),
+            pltpu.VMEM((slots, model), BF16),
             pltpu.VMEM((2, slots, ff), BF16),
             pltpu.VMEM((4, rows, model), BF16),
             pltpu.VMEM((6, rows, model), BF16),
             pltpu.VMEM((rows, model), F32),
-            pltpu.VMEM((rows, model), BF16),
             dma((2,)),
             dma((3,)),
             dma((depth - 1, CHUNKS)),
@@ -1090,7 +1118,6 @@
             dma((depth, CHUNKS)),
             dma((1,)),
             dma((6, CHUNKS)),
-            dma((1,)),
         ],
         compiler_params=pltpu.CompilerParams(
             collective_id=0, has_side_effects=True, vmem_limit_bytes=56 * 1024 * 1024

time: 126 us -> 119 us (0.944)
  Pallas kernels: 124 us -> 118 us
    pallas_call x1, Pallas kernels: 124 us -> 118 us  [on_device(): pl.pallas_call(functools.partial(layer_kernel, n, dp, capacity), out_shap...]
where the time goes in v5:
time: 119 us
  Pallas kernels  118 us (99%)
    pallas_call x1, Pallas kernels, on_device(): pl.pallas_call(functools.partial(layer_kernel, n, dp, capacity), out_shap...  118 us

profile of v5, /device:TPU:8, one launch (start us, length us, event | category | flops | bytes accessed | tf_op | source)
XLA Modules:
  0.0 119.3 jit_solution(17787277959050584766)
XLA Ops:
  0.0 118.5 %layer.1 = bf16[128,2048]{1,0:T(8,128)(2,1)S(1)} custom-call(bf16[128,16,128]{2,1,0:T(8,128)(2,1)} %bitcast.15, bf16[128,4,128]{2,1,0:T(4,128)(2,1)} %bitcast.17, bf16[128,4,128]{2,1,0:T(4,128)(2,1)} %bitcast.18, f32[1,128]{1,0:T(1,128)} %bitcast.22, f32[1,128]{1,0:T(1,128)} %bitcast.23, bf16[256,512]{1,0:T(8,128)(2,1)} %refs_5_.1, ...), custom_call_target="tpu_custom_call" | custom-call | tf_op jit(solution)/shard_map/layer/pallas_call | solution.py:1085
  118.5 0.8 copy.15

commit v6 on v5

--- a/solution.py
+++ b/solution.py
@@ -158,6 +158,7 @@
     w_full,
     swap,
     att,
+    total,
     proj,
     back,
     res_in,
@@ -337,6 +338,11 @@
                 kv_line.down(always, u, z)
     fetches[5].wait()
 
+    far = depth - 1 - z
+
+    def is_far(plane):
+        return jnp.where(plane == far, 1, 0)
+
     def w_across(condition, u, plane):
         for k in range(1, across):
 
@@ -346,7 +352,7 @@
                     w_unit(u, plane * across + x),
                     w_unit(u, plane * across + x),
                     wx_send.at[w_units[u][0]],
-                    wx_recv.at[w_units[u][0]] if plane is not z else wo_sem.at[0],
+                    wx_recv.at[w_units[u][0], is_far(plane)] if plane is not z else wo_sem.at[0],
                     sp=beside(k),
                 ).start()
 
@@ -370,14 +376,16 @@
             for k in range(1, across):
                 block = w_half(beside(k), j)
                 target = me + way * across
-                remote(block, block, wo_sem.at[1], wx_recv.at[j], sp=target).start()
-
+                inner = jnp.where(middle, 1, 0)
+                remote(block, block, wo_sem.at[1], wx_recv.at[j, inner], sp=target).start()
+
+    def w_back():
         @pl.when(middle)
         def _():
             for k in range(1, across):
                 block = w_half(beside(k), 0)
                 target = me - way * across
-                remote(block, block, wo_sem.at[2], wx_recv.at[0], sp=target).start()
+                remote(block, block, wo_sem.at[2], wx_recv.at[0, 0], sp=target).start()
 
     def w_aside(units):
         def then(condition, u, plane):
@@ -478,6 +486,7 @@
     for t in range(2, depth - 1):
         for u in range(len(w_units)):
             w_line.step(t, u, middle, w_across)
+    w_back()
     for u in range(len(w_units)):
         w_line.step(1, u, edge, w_aside((1,)))
     for u, (k, g) in enumerate(kv_units):
@@ -510,13 +519,32 @@
         ).wait_recv()
     remote(att.at[mine], att.at[mine], pair_sem.at[0], pair_sem.at[1], dp=mine).wait_recv()
 
+    deep = across * w_rows
+
+    def project(place, cols):
+        lines = pl.ds(pl.multiple_of(place * deep, deep), deep)
+        return jnp.dot(
+            att[:, :, lines].reshape(dp * rows, deep),
+            w_full[lines, cols],
+            preferred_element_type=F32,
+        )
+
+    def w_wait(j, planes, which):
+        block = w_full.at[
+            pl.ds(0, planes * (across - 1) * w_rows), pl.ds(j * part_cols, part_cols)
+        ]
+        remote(block, block, wx_send.at[0], wx_recv.at[j, which], sp=me).wait_recv()
+
     for j in range(halves):
         cols = slice(j * part_cols, (j + 1) * part_cols)
-        block = w_full.at[pl.ds(0, (depth - 1) * (across - 1) * w_rows), cols]
-        remote(block, block, wx_send.at[0], wx_recv.at[j], sp=me).wait_recv()
-        result = jnp.dot(
-            att[...].reshape(dp * rows, model), w_full[:, cols], preferred_element_type=F32
-        ).astype(BF16)
+        w_wait(j, depth - 2, 0)
+        total[:, cols] = project(lax.rem(far + 1, depth), cols)
+        for step in range(2, depth):
+            total[:, cols] += project(lax.rem(far + step, depth), cols)
+    for j in range(halves):
+        cols = slice(j * part_cols, (j + 1) * part_cols)
+        w_wait(j, 1, 1)
+        result = (total[:, cols] + project(far, cols)).astype(BF16)
         for s in range(dp):
             proj[s, :, cols] = result[s * rows : (s + 1) * rows]
         back[mine, :, cols] = proj[mine, :, cols]
@@ -905,18 +933,20 @@
         toward(1, 3)
         ask(2, 3)
         ask(3, 0)
+        ask(3, 1)
         self.serve_up(0)
-        ask(3, 1)
+        ask(3, 2)
         self.serve_up(2)
         down(2, *chunks)
-        ask(3, 2)
         ask(3, 3)
         for c in chunks:
             toward(2, c)
+        down(0, 0, 1)
         self.serve_up(3)
         down(3, *chunks)
-        down(0, *chunks)
-        for c in chunks:
+        toward(3, 0)
+        down(0, 2, 3)
+        for c in range(1, CHUNKS):
             toward(3, c)
         for c in chunks:
             self.own(c)
@@ -929,11 +959,12 @@
 
         def down(r, *cs):
             for c in cs:
-                self.serve_down(r, c, r == 0 and c == 0)
+                self.serve_down(r, c, r == 1 and c == 0)
 
         for c in chunks:
             ask(0, c)
         ask(3, 0)
+        ask(3, 1)
         ask(1, 0)
         ask(1, 1)
         ask(2, 0)
@@ -942,26 +973,26 @@
         ask(1, 3)
         ask(2, 2)
         ask(2, 3)
-        ask(3, 1)
         ask(3, 2)
         ask(3, 3)
-        for r in (0, 1, 2, 3):
-            self.serve_up(r, r == 0)
+        for r in (1, 2, 3):
+            self.serve_up(r, r == 1)
             down(r, *chunks)
+        self.serve_up(0)
+
+        def far(c):
+            self.merge(2, c, 1, 3, 1, 1)
+
+        def near(c):
+            self.merge(1, c, 3, 5, -1, 3)
+
+        for c in chunks:
+            far(c)
+        down(0, *chunks)
+        for c in chunks:
+            near(c)
         for c in chunks:
             self.own(c)
-
-        def far(c):
-            self.merge(2, c, 1, 3, 1, 1)
-
-        def near(c):
-            self.merge(1, c, 3, 5, -1, 3)
-
-        for c in chunks:
-            far(c)
-            if c > 0:
-                near(c - 1)
-        near(CHUNKS - 1)
         for c in chunks:
             self.merge(3, c, 2, 4, 1, 2)
         for c in chunks:
@@ -993,7 +1024,7 @@
     inputs, refs = refs[:10], refs[10:]
     weights, out_ref, refs = refs[:3], refs[3], refs[4:]
     middle, refs = refs[:2], refs[2:]
-    attention, refs = refs[:36], refs[36:]
+    attention, refs = refs[:37], refs[37:]
     load_sem, stores = refs[0], refs[1:4]
     loads = [
         pltpu.make_async_copy(src.at[0], dst, load_sem.at[i])
@@ -1004,7 +1035,7 @@
         for load in loads:
             load.start()
 
-    norm = attention[15]
+    norm = attention[16]
     experts = Experts(n, dp, capacity, norm, *inputs[8:], middle, loads, out_ref, *refs[1:])
     drain = attention_part(n, dp, start_loads, *inputs[:8], *middle, experts, *attention)
     experts.run()
@@ -1056,6 +1087,7 @@
         pltpu.VMEM((w_rows * n, w_cols), BF16),
         pltpu.VMEM((across - 1, rows, local * width), BF16),
         pltpu.VMEM((dp, rows, model), BF16),
+        pltpu.VMEM((dp * rows, w_cols), F32),
         pltpu.VMEM((dp, rows, w_cols), BF16),
         pltpu.VMEM((dp, rows, w_cols), BF16),
         pltpu.VMEM((rows, model), BF16),
@@ -1069,7 +1101,7 @@
         dma((1,)),
         dma((1,)),
         dma((2,)),
-        dma((2,)),
+        dma((2, 2)),
         dma((3,)),
         dma((2,)),
         dma((4, depth)),

time: 119 us -> 117 us (0.983)
  Pallas kernels: 118 us -> 116 us
    pallas_call x1, Pallas kernels: 118 us -> 116 us  [on_device(): pl.pallas_call(functools.partial(layer_kernel, n, dp, capacity), out_shap...]
where the time goes in v6:
time: 117 us
  Pallas kernels  116 us (99%)
    pallas_call x1, Pallas kernels, on_device(): pl.pallas_call(functools.partial(layer_kernel, n, dp, capacity), out_shap...  116 us

profile of v6, /device:TPU:8, one launch (start us, length us, event | category | flops | bytes accessed | tf_op | source)
XLA Modules:
  0.0 116.7 jit_solution(18072416575074649998)
XLA Ops:
  0.0 115.9 %layer.1 = bf16[128,2048]{1,0:T(8,128)(2,1)S(1)} custom-call(bf16[128,16,128]{2,1,0:T(8,128)(2,1)} %bitcast.15, bf16[128,4,128]{2,1,0:T(4,128)(2,1)} %bitcast.17, bf16[128,4,128]{2,1,0:T(4,128)(2,1)} %bitcast.18, f32[1,128]{1,0:T(1,128)} %bitcast.22, f32[1,128]{1,0:T(1,128)} %bitcast.23, bf16[256,512]{1,0:T(8,128)(2,1)} %refs_5_.1, ...), custom_call_target="tpu_custom_call" | custom-call | tf_op jit(solution)/shard_map/layer/pallas_call | solution.py:1117
  115.9 0.8 copy.15

commit v7 on v6

--- a/solution.py
+++ b/solution.py
@@ -934,20 +934,18 @@
         ask(2, 3)
         ask(3, 0)
         ask(3, 1)
-        self.serve_up(0)
         ask(3, 2)
         self.serve_up(2)
         down(2, *chunks)
         ask(3, 3)
         for c in chunks:
             toward(2, c)
-        down(0, 0, 1)
         self.serve_up(3)
         down(3, *chunks)
-        toward(3, 0)
-        down(0, 2, 3)
-        for c in range(1, CHUNKS):
+        for c in chunks:
             toward(3, c)
+        self.serve_up(0)
+        down(0, *chunks)
         for c in chunks:
             self.own(c)
         for c in chunks:

time: 117 us -> 117 us (level)
  no operation moved by 1% of the time
where the time goes in v7:
time: 117 us; the launch traced here: 116 us
  Pallas kernels  115 us (98%)
    pallas_call x1, Pallas kernels, on_device(): pl.pallas_call(functools.partial(layer_kernel, n, dp, capacity), out_shap...  115 us

profile of v7, /device:TPU:8, one launch (start us, length us, event | category | flops | bytes accessed | tf_op | source)
XLA Modules:
  0.0 116.2 jit_solution(480446058735835368)
XLA Ops:
  0.0 115.4 %layer.1 = bf16[128,2048]{1,0:T(8,128)(2,1)S(1)} custom-call(bf16[128,16,128]{2,1,0:T(8,128)(2,1)} %bitcast.15, bf16[128,4,128]{2,1,0:T(4,128)(2,1)} %bitcast.17, bf16[128,4,128]{2,1,0:T(4,128)(2,1)} %bitcast.18, f32[1,128]{1,0:T(1,128)} %bitcast.22, f32[1,128]{1,0:T(1,128)} %bitcast.23, bf16[256,512]{1,0:T(8,128)(2,1)} %refs_5_.1, ...), custom_call_target="tpu_custom_call" | custom-call | tf_op jit(solution)/shard_map/layer/pallas_call | solution.py:1115
  115.4 0.8 copy.15
